TPU v7x, 512 devices: a whole 4x8x8 slice. The times are simulated.
512 devices in a mesh: sp: 64 (over z, y), tp: 8 (over x, core).
Axes of the slice: x: 4, y: 8, z: 8, core: 2. Of those that a mesh axis runs over, the one named last changes fastest.
Arguments:
- latent: bfloat16 [32768, 2048], P(('sp', 'tp')), may hold values from -6 to 6
- context: bfloat16 [1024, 2048], P('sp'), may hold values from -6 to 6
- condition: float32 [2048], replicated, may hold values from -6 to 6
- context_condition: float32 [2048], replicated, may hold values from -6 to 6
- modulation_weight: bfloat16 [2048, 3, 2048], P('sp', None, 'tp'), may hold values from -0.125 to 0.125
- norm_gain: float32 [2048], replicated, may hold values from 0.1 to 1.9
- query_weight: bfloat16 [2048, 2048], P(None, 'tp'), may hold values from -0.125 to 0.125
- key_weight: bfloat16 [2048, 2048], P(None, 'tp'), may hold values from -0.125 to 0.125
- value_weight: bfloat16 [2048, 2048], P(None, 'tp'), may hold values from -0.125 to 0.125
- log_decay: float32 [2, 32], P(None, 'tp')
- head_gain: float32 [2048], P('tp'), may hold values from 0.1 to 1.9
- output_weight: bfloat16 [2048, 2048], P('sp'), may hold values from -0.125 to 0.125
Outputs:
- output: bfloat16 [32768, 2048], P(('sp', 'tp'))
All inputs are finite; a program needn't handle non-finite values.
Results may differ from a plain program's by a relative error of at most 0.0065.
Values may be sent and summed in bfloat16 or wider, within the bound.
A program may use at most 128 MiB of HBM per device.

v0:
```python
import functools

import jax
import jax.numpy as jnp
from jax import lax
from jax.sharding import Mesh
from jax.sharding import PartitionSpec as P

D = 2048
HEAD = 64
BLOCK = 128
CTX = 1024
SP = ("sp_0", "sp_1")
TP = ("tp_0", "tp_1")
SP_TP = ("sp_0", "sp_1", "tp_0", "tp_1")


EPSILON = 1e-06
ROTARY_BASE = 10000.0
MAXIMAL_ACCURACY = lax.Precision.HIGHEST


def over_axes(shard, axes):
    return functools.reduce(lax.psum, axes, shard)


def copy_for_each(shard, axis):
    devices = lax.axis_size(axis)
    return lax.all_to_all(
        jnp.broadcast_to(shard[None], (devices, *shard.shape)), axis, 0, 0, tiled=True
    )


def joined_along(blocks, dim):
    dims = list(blocks.shape[1:])
    dims[dim] *= blocks.shape[0]
    return jnp.moveaxis(blocks, 0, dim).reshape(dims)


def gathered_copies(shard, axis, dim):
    blocks = copy_for_each(shard, axis)
    return joined_along(blocks, dim)


def nothing_yet(shard, identity):
    return jax.tree.map(
        lambda a, e: jnp.broadcast_to(jnp.asarray(e, a.dtype), a.shape), shard, identity
    )


def collected_together(shard, axis):
    leaves = jax.tree.leaves(shard)
    order = sorted(range(len(leaves)), key=lambda k: -leaves[k].size)
    width = (1, *leaves[order[0]].shape)[-1]
    lines = [
        jnp.pad(leaves[k].reshape(-1), (0, -leaves[k].size % width)).reshape(-1, width)
        for k in order
    ]
    both, at, found = (lax.all_gather(jnp.concatenate(lines), axis), 0, {})
    for k, line in zip(order, lines):
        section = both[:, at : at + len(line)].reshape(len(both), -1)
        found[k] = section[:, : leaves[k].size].reshape(-1, *leaves[k].shape)
        at += len(line)
    numbers = iter(range(len(leaves)))
    return jax.tree.map(lambda _: found[next(numbers)], shard)


def carried_in(shard, axes, combine, identity, reverse):
    before = start = nothing_yet(shard, identity)
    so_far = shard
    for axis in reversed(axes):
        devices, here = (lax.axis_size(axis), lax.axis_index(axis))
        pieces = collected_together(so_far, axis)
        inside, so_far = (start, start)
        for k in reversed(range(devices)) if reverse else range(devices):
            passed = k > here if reverse else k < here
            so_far = combine(so_far, jax.tree.map(lambda part: part[k], pieces))
            inside = jax.tree.map(lambda new, old: jnp.where(passed, new, old), so_far, inside)
        before = combine(inside, before)
    return before


def rotation_tables(positions):
    half_size = HEAD // 2
    frequency = 1.0 / ROTARY_BASE ** jnp.linspace(0.0, 1.0, half_size, dtype=jnp.float32)
    angles = positions[:, None] * frequency[None, :]
    return (jnp.cos(angles), jnp.sin(angles))


def rotate(projected, positions):
    cos_table, sin_table = rotation_tables(positions)
    half_size = HEAD // 2
    lower_half = projected[..., :half_size]
    upper_half = projected[..., half_size:]
    cos_table = cos_table[:, None, :]
    sin_table = sin_table[:, None, :]
    return jnp.concatenate(
        [
            lower_half * cos_table - upper_half * sin_table,
            lower_half * sin_table + upper_half * cos_table,
        ],
        axis=-1,
    )


def modulated(rows, gain, shift, scale):
    widened = rows.astype(jnp.float32)
    scaled = widened * lax.rsqrt(jnp.mean(widened * widened, axis=-1, keepdims=True) + EPSILON)
    return (scaled * gain * (1.0 + scale) + shift).astype(jnp.bfloat16)


def context_states(projected, log_decay):
    width = projected.shape[1] // 2
    head_count = width // HEAD
    length = projected.shape[0]
    positions = jnp.arange(length, dtype=jnp.float32)
    keys = rotate(projected[:, :width].reshape(length, head_count, HEAD), positions).astype(
        jnp.bfloat16
    )
    values = projected[:, width:].reshape(length, head_count, HEAD).astype(jnp.bfloat16)
    broad_key_matrix = keys.astype(jnp.float32)
    broad_value_matrix = values.astype(jnp.float32)
    forward_weight = jnp.exp(log_decay[0][None, :] * (CTX - 1.0 - positions)[:, None])
    backward_weight = jnp.exp(log_decay[1][None, :] * positions[:, None])
    forward_state = jnp.einsum(
        "jhd,jhe->hde",
        broad_key_matrix * forward_weight[:, :, None],
        broad_value_matrix,
        precision=MAXIMAL_ACCURACY,
    )
    backward_state = jnp.einsum(
        "jhd,jhe->hde",
        broad_key_matrix * backward_weight[:, :, None],
        broad_value_matrix,
        precision=MAXIMAL_ACCURACY,
    )
    return (forward_state, backward_state)


def local_sweep(queries, keys, values, log_rate):
    length, head_count, head_size = queries.shape
    blocks = length // BLOCK
    offsets = jnp.arange(BLOCK, dtype=jnp.float32)
    distance = offsets[:, None] - offsets[None, :]
    decay_mask = jnp.where(
        distance >= 0, jnp.exp(log_rate[:, None, None] * jnp.maximum(distance, 0.0)[None]), 0.0
    )
    query_decay = jnp.exp(log_rate[:, None] * (offsets + 1.0)[None]).T
    key_decay = jnp.exp(log_rate[:, None] * (BLOCK - 1.0 - offsets)[None]).T
    block_decay = jnp.exp(log_rate * BLOCK)
    query_blocks = queries.reshape(blocks, BLOCK, head_count, head_size)
    key_blocks = keys.reshape(blocks, BLOCK, head_count, head_size)
    value_blocks = values.reshape(blocks, BLOCK, head_count, head_size)
    affinity_scores = jnp.einsum(
        "blhd,bmhd->bhlm", query_blocks, key_blocks, preferred_element_type=jnp.float32
    )
    weight_tensors = (affinity_scores * decay_mask[None]).astype(jnp.bfloat16)
    inside_block = jnp.einsum(
        "bhlm,bmhd->blhd", weight_tensors, value_blocks, preferred_element_type=jnp.float32
    )
    updates = jnp.einsum(
        "blhd,blhe->bhde",
        key_blocks.astype(jnp.float32) * key_decay[None, :, :, None],
        value_blocks.astype(jnp.float32),
        precision=MAXIMAL_ACCURACY,
    )

    def carry_step(state, update):
        return (block_decay[:, None, None] * state + update, state)

    final_state, prior_state = lax.scan(
        carry_step, jnp.zeros((head_count, head_size, head_size), jnp.float32), updates
    )
    carried = (
        jnp.einsum(
            "blhd,bhde->blhe",
            query_blocks.astype(jnp.float32),
            prior_state,
            precision=MAXIMAL_ACCURACY,
        )
        * query_decay[None, :, :, None]
    )
    return ((inside_block + carried).reshape(length, head_count, head_size), final_state)


def incoming(queries, entering, log_rate):
    length = queries.shape[0]
    factor = jnp.exp(log_rate[None, :] * (jnp.arange(length, dtype=jnp.float32) + 1.0)[:, None])
    return (
        jnp.einsum(
            "thd,hde->the", queries.astype(jnp.float32), entering, precision=MAXIMAL_ACCURACY
        )
        * factor[:, :, None]
    )


def combine(earlier, later):
    return (earlier[0] * later[0], later[0][:, None, None] * earlier[1] + later[1])


def per_device(
    latent,
    context,
    condition,
    context_condition,
    modulation_weight,
    norm_gain,
    query_weight,
    key_weight,
    value_weight,
    log_decay,
    head_gain,
    output_weight,
):
    seq_count = lax.axis_size(SP)
    seq_index = lax.axis_index(SP)
    tp_count = lax.axis_size(TP)
    tp_index = lax.axis_index(TP)
    activated = jax.nn.silu(jnp.stack([condition, context_condition])).astype(jnp.bfloat16)
    row_count = modulation_weight.shape[0]
    col_count = modulation_weight.shape[2]
    own_inputs = lax.dynamic_slice_in_dim(activated, seq_index * row_count, row_count, 1)
    partial_mod = jnp.dot(
        own_inputs,
        modulation_weight.reshape(row_count, 3 * col_count),
        preferred_element_type=jnp.float32,
    ).reshape(2, 3, col_count)
    padded = lax.dynamic_update_slice_in_dim(
        jnp.zeros((2, 3, D), jnp.float32), partial_mod, tp_index * col_count, 2
    )
    modulation = over_axes(padded, SP_TP)
    normed = modulated(latent, norm_gain, modulation[0, 0], modulation[0, 1])
    tok_dev = latent.shape[0] * tp_count
    width = query_weight.shape[1]
    head_count = width // HEAD
    projection = jnp.concatenate([query_weight, key_weight, value_weight], axis=1)
    projected = jnp.dot(
        gathered_copies(normed, TP, 0), projection, preferred_element_type=jnp.float32
    )
    positions = (
        CTX + (seq_index * tok_dev).astype(jnp.float32) + jnp.arange(tok_dev, dtype=jnp.float32)
    )
    queries = (
        rotate(projected[:, :width].reshape(tok_dev, head_count, HEAD), positions) * HEAD ** (-0.5)
    ).astype(jnp.bfloat16)
    keys = rotate(
        projected[:, width : 2 * width].reshape(tok_dev, head_count, HEAD), positions
    ).astype(jnp.bfloat16)
    values = projected[:, 2 * width :].reshape(tok_dev, head_count, HEAD).astype(jnp.bfloat16)
    context_normed = modulated(context, norm_gain, modulation[1, 0], modulation[1, 1])
    pair_weight = jnp.concatenate([key_weight, value_weight], axis=1)
    empty_state = jnp.zeros((head_count, HEAD, HEAD), jnp.float32)
    start_forward, start_backward = context_states(
        jnp.dot(
            lax.all_gather(context_normed, SP, axis=0, tiled=True),
            pair_weight,
            preferred_element_type=jnp.float32,
        ),
        log_decay,
    )
    forward_local, forward_final = local_sweep(queries, keys, values, log_decay[0])
    reversed_queries = jnp.flip(queries, 0)
    backward_local, backward_final = local_sweep(
        reversed_queries, jnp.flip(keys, 0), jnp.flip(values, 0), log_decay[1]
    )
    identity = (jnp.ones((head_count,), jnp.float32), empty_state)
    forward_span = jnp.exp(log_decay[0] * tok_dev)
    backward_span = jnp.exp(log_decay[1] * tok_dev)
    forward_prefix = carried_in((forward_span, forward_final), SP, combine, identity, False)
    backward_prefix = carried_in((backward_span, backward_final), SP, combine, identity, True)
    enter_forward = forward_prefix[1]
    enter_backward = backward_prefix[1]
    before_count = (seq_index * tok_dev).astype(jnp.float32)
    after_count = ((seq_count - 1 - seq_index) * tok_dev).astype(jnp.float32)
    enter_forward = (
        enter_forward + jnp.exp(log_decay[0] * before_count)[:, None, None] * start_forward
    )
    enter_backward = (
        enter_backward + jnp.exp(log_decay[1] * after_count)[:, None, None] * start_backward
    )
    forward = forward_local + incoming(queries, enter_forward, log_decay[0])
    backward = jnp.flip(
        backward_local + incoming(reversed_queries, enter_backward, log_decay[1]), 0
    )
    combined = forward + backward
    centre = jnp.mean(combined, axis=-1, keepdims=True)
    spread = jnp.mean(jnp.square(combined - centre), axis=-1, keepdims=True)
    retained = (
        (combined - centre) * lax.rsqrt(spread + EPSILON) * head_gain.reshape(head_count, HEAD)
    ).astype(jnp.bfloat16)
    retained = retained.reshape(tok_dev, width)
    own_rows = lax.all_to_all(retained, TP, split_axis=0, concat_axis=1, tiled=True)
    mixed = jnp.dot(
        own_rows,
        lax.all_gather(output_weight, SP, axis=0, tiled=True),
        preferred_element_type=jnp.float32,
    )
    return (latent.astype(jnp.float32) + modulation[0, 2] * mixed).astype(jnp.bfloat16)


def solution(mesh):
    split = Mesh(mesh.devices.reshape(8, 8, 4, 2), ("sp_0", "sp_1", "tp_0", "tp_1"))
    placed = (
        P(SP_TP, None),
        P(SP, None),
        P(),
        P(),
        P(SP, None, TP),
        P(),
        P(None, TP),
        P(None, TP),
        P(None, TP),
        P(None, TP),
        P(TP),
        P(SP, None),
    )
    return jax.shard_map(
        per_device, mesh=split, in_specs=placed, out_specs=P(SP_TP, None), check_vma=False
    )
```

profile of v0, /device:TPU:1, one launch (start us, length us, event | category | flops | bytes accessed | tf_op | source)
XLA Modules:
  0.0 343.8 jit_solution(15762004507316060974)
XLA Ops:
  8.2 30.1 %psum.28 = f32[2,3,2048]{2,0,1:T(2,128)S(1)} all-reduce(f32[2,3,2048]{2,0,1:T(2,128)S(1)} %convolution_dynamic-update-slice_fusion), channel_id=1, replica_groups=mesh['sp_0'=8,'sp_1'=8,'tp_0'=4,'tp_1'=2] {'sp_0'}, use_global_device_ids=true, to_apply=%region_0.1 | all-reduce | flops 12288 | bytes 98304 | tf_op jit(solution)/shard_map/psum | solution.py:24
  38.3 23.6 %psum.29 = f32[2,3,2048]{2,0,1:T(2,128)S(1)} all-reduce(f32[2,3,2048]{2,0,1:T(2,128)S(1)} %psum.28), channel_id=1, replica_groups=mesh['sp_0'=8,'sp_1'=8,'tp_0'=4,'tp_1'=2] {'sp_1'}, use_global_device_ids=true, to_apply=%region_1.2 | all-reduce | flops 12288 | bytes 98304 | tf_op jit(solution)/shard_map/psum | solution.py:24
  61.9 13.6 %psum.30 = f32[2,3,2048]{2,0,1:T(2,128)S(1)} all-reduce(f32[2,3,2048]{2,0,1:T(2,128)S(1)} %psum.29), channel_id=1, replica_groups=mesh['sp_0'=8,'sp_1'=8,'tp_0'=4,'tp_1'=2] {'tp_0'}, use_global_device_ids=true, to_apply=%region_2.3 | all-reduce | flops 12288 | bytes 98304 | tf_op jit(solution)/shard_map/psum | solution.py:24
  75.5 22.1 %psum.31 = f32[2,3,2048]{2,0,1:T(2,128)S(1)} all-reduce(f32[2,3,2048]{2,0,1:T(2,128)S(1)} %psum.30), channel_id=1, replica_groups=mesh['sp_0'=8,'sp_1'=8,'tp_0'=4,'tp_1'=2] {'tp_1'}, use_global_device_ids=true, to_apply=%region_3.4 | all-reduce | flops 12288 | bytes 98304 | tf_op jit(solution)/shard_map/psum | solution.py:24
  99.2 1.6 fusion.68
  103.1 1.6 broadcast_in_dim.22
  104.7 3.7 %all-to-all-start = ((bf16[8,64,2048]{2,1,0:T(8,128)(2,1)}), bf16[8,64,2048]{2,1,0:T(8,128)(2,1)S(1)}, u32[]{:S(2)}, u32[]{:S(2)}) async-start(bf16[8,64,2048]{2,1,0:T(8,128)(2,1)} %broadcast_in_dim.22), calls=%async_computation | async-start | bytes 4194304 | tf_op jit(solution)/shard_map/all_to_all | solution.py:29
  115.4 19.2 %all-to-all-done = bf16[8,64,2048]{2,1,0:T(8,128)(2,1)S(1)} async-done(((bf16[8,64,2048]{2,1,0:T(8,128)(2,1)}), bf16[8,64,2048]{2,1,0:T(8,128)(2,1)S(1)}, u32[]{:S(2)}, u32[]{:S(2)}) %all-to-all-start) | async-done | bytes 2097184 | tf_op jit(solution)/shard_map/all_to_all | solution.py:29
  134.6 3.6 %fusion = f32[512,768]{1,0:T(8,128)S(1)} fusion(bf16[512,2048]{1,0:T(8,128)(2,1)S(1)} %bitcast.514, bf16[2048,256]{1,0:T(8,128)(2,1)} %param.26, bf16[2048,256]{1,0:T(8,128)(2,1)} %param.25, bf16[2048,256]{1,0:T(8,128)(2,1)} %param.24), kind=kOutput, calls=%fused_computation.4 | convolution fusion | flops 1620049920 | bytes 6815744 | tf_op jit(solution)/shard_map/dot_general | solution.py:237
  142.1 22.9 %all-gather.6 = f32[8,257,64]{1,2,0:T(8,128)S(1)} all-gather(f32[1,257,64]{1,2,0:T(8,128)S(1)} %maximum_bitcast_fusion.2), channel_id=4, replica_groups=mesh['sp_0'=8,'sp_1'=8,'tp_0'=4,'tp_1'=2] {'sp_1'}, dimensions={0}, use_global_device_ids=true | all-gather | bytes 592128 | tf_op jit(solution)/shard_map/all_gather | solution.py:59
  165.7 1.6 copy.286
  175.1 20.3 %all-gather.7 = f32[8,257,64]{1,2,0:T(8,128)S(1)} all-gather(f32[1,257,64]{1,2,0:T(8,128)S(1)} %maximum_bitcast_fusion.3), channel_id=5, replica_groups=mesh['sp_0'=8,'sp_1'=8,'tp_0'=4,'tp_1'=2] {'sp_0'}, dimensions={0}, use_global_device_ids=true | all-gather | bytes 592128 | tf_op jit(solution)/shard_map/all_gather | solution.py:59
  204.3 3.0 while.26
  207.5 21.3 %all-gather.4 = f32[8,257,64]{1,2,0:T(8,128)S(1)} all-gather(f32[1,257,64]{1,2,0:T(8,128)S(1)} %maximum_bitcast_fusion), channel_id=2, replica_groups=mesh['sp_0'=8,'sp_1'=8,'tp_0'=4,'tp_1'=2] {'sp_1'}, dimensions={0}, use_global_device_ids=true | all-gather | bytes 592128 | tf_op jit(solution)/shard_map/all_gather | solution.py:59
  230.3 1.6 copy.255
  231.9 1.6 copy.254
  233.5 1.6 copy.253
  235.1 1.6 copy.252
  236.6 1.6 copy.251
  238.2 1.6 copy.250
  239.8 1.6 copy.249
  246.2 26.3 %all-gather.5 = f32[8,257,64]{1,2,0:T(8,128)S(1)} all-gather(f32[1,257,64]{1,2,0:T(8,128)S(1)} %maximum_bitcast_fusion.1), channel_id=3, replica_groups=mesh['sp_0'=8,'sp_1'=8,'tp_0'=4,'tp_1'=2] {'sp_0'}, dimensions={0}, use_global_device_ids=true | all-gather | bytes 592128 | tf_op jit(solution)/shard_map/all_gather | solution.py:59
  273.3 1.6 copy.247
  274.9 1.6 copy.246
  276.5 1.6 copy.245
  282.0 1.6 fusion.23
  285.8 1.6 fusion.20
  288.6 5.2 %fusion.8 = f32[1024,512]{0,1:T(8,128)S(1)} fusion(bf16[1024,2048]{1,0:T(8,128)(2,1)} %all-gather.11.cloned.1.call-done, bf16[2048,256]{1,0:T(8,128)(2,1)} %param.26, bf16[2048,256]{1,0:T(8,128)(2,1)} %param.25), kind=kOutput, calls=%fused_computation.13 | convolution fusion | flops 2151677952 | bytes 8388608 | tf_op jit(solution)/shard_map/dot_general | solution.py:254
  295.8 1.6 fusion.25
  298.5 2.5 fusion.26
  302.4 28.7 %all_to_all.24 = bf16[8,64,256]{2,1,0:T(8,128)(2,1)S(1)} all-to-all(bf16[8,64,256]{2,1,0:T(8,128)(2,1)S(1)} %copy.288), channel_id=1, replica_groups=mesh['sp_0'=8,'sp_1'=8,'tp_0'=4,'tp_1'=2] {'tp_0','tp_1'}, dimensions={0} | all-to-all | bytes 524288 | tf_op jit(solution)/shard_map/all_to_all | solution.py:292
  331.3 5.7 %fusion.7 = bf16[64,2048]{1,0:T(8,128)(2,1)} fusion(bf16[64,2048]{1,0:T(8,128)(2,1)S(1)} %bitcast.517, bf16[2048,2048]{1,0:T(8,128)(2,1)} %all-gather.13.cloned.1.call-done, bf16[64,2048]{1,0:T(8,128)(2,1)S(1)} %copy-done.1, f32[2048]{0:T(1024)S(1)} %bitcast.557), kind=kOutput, calls=%fused_computation.12 | convolution fusion | flops 537395200 | bytes 9183232 | tf_op jit(solution)/shard_map/dot_general | solution.py:293
  (308 shorter events, 54.9 us)
Async XLA Ops:
  6.5 282.1 %all-gather.11.cloned.1.call-start = ((), (), s32[]{:S(2)}) async-start(), calls=%async_computation.2 | async-start | bytes 4259840 | tf_op jit(solution)/shard_map/all_gather | solution.py:255
  103.1 6.1 %copy-start.40 = (f32[2,4]{1,0:T(2,128)S(1)}, f32[2,4]{1,0:T(2,128)}, u32[]{:S(2)}) copy-start(f32[2,4]{1,0:T(2,128)} %param.27) | copy-start | bytes 100
  103.1 7.0 %copy-start.61 = (f32[256]{0:T(256)S(1)}, f32[256]{0:T(256)}, u32[]{:S(2)}) copy-start(f32[256]{0:T(256)} %param.28) | copy-start | bytes 3076
  104.7 29.9 %all-to-all-start = ((bf16[8,64,2048]{2,1,0:T(8,128)(2,1)}), bf16[8,64,2048]{2,1,0:T(8,128)(2,1)S(1)}, u32[]{:S(2)}, u32[]{:S(2)}) async-start(bf16[8,64,2048]{2,1,0:T(8,128)(2,1)} %broadcast_in_dim.22), calls=%async_computation | async-start | bytes 4194304 | tf_op jit(solution)/shard_map/all_to_all | solution.py:29
  108.4 222.9 %all-gather.13.cloned.1.call-start = ((), (), s32[]{:S(2)}) async-start(), calls=%async_computation.3 | async-start | bytes 8519680 | tf_op jit(solution)/shard_map/all_gather | solution.py:295
  175.1 27.7 %copy-start.6 = (bf16[512,4,32]{0,2,1:T(8,128)(2,1)S(1)}, bf16[512,4,32]{0,2,1:T(8,128)(2,1)}, u32[]{:S(2)}) copy-start(bf16[512,4,32]{0,2,1:T(8,128)(2,1)} %copy-done.5) | copy-start | bytes 393220
  175.1 27.7 %copy-start.4 = (bf16[512,4,32]{0,2,1:T(8,128)(2,1)S(1)}, bf16[512,4,32]{0,2,1:T(8,128)(2,1)}, u32[]{:S(2)}) copy-start(bf16[512,4,32]{0,2,1:T(8,128)(2,1)} %copy-done.3) | copy-start | bytes 393220
  175.1 27.8 %copy-start.38 = (f32[128,4]{0,1:T(4,128)S(1)}, f32[128,4]{0,1:T(4,128)}, u32[]{:S(2)}) copy-start(f32[128,4]{0,1:T(4,128)} %get-tuple-element.220) | copy-start | bytes 6148
  195.5 8.8 %copy-start.32 = (f32[4]{0:T(128)S(1)}, f32[4]{0:T(128)}, u32[]{:S(2)}) copy-start(f32[4]{0:T(128)} %get-tuple-element.321) | copy-start | bytes 52
  243.2 38.8 %copy-start.37 = (f32[128,4]{0,1:T(4,128)S(1)}, f32[128,4]{0,1:T(4,128)}, u32[]{:S(2)}) copy-start(f32[128,4]{0,1:T(4,128)} %get-tuple-element.219) | copy-start | bytes 6148
  272.6 11.1 %copy-start.7 = (f32[4,128,128]{2,1,0:T(8,128)S(1)}, f32[4,128,128]{2,1,0:T(8,128)}, u32[]{:S(2)}) copy-start(f32[4,128,128]{2,1,0:T(8,128)} %get-tuple-element.168) | copy-start | bytes 786436
  278.1 7.1 %copy-start.36 = (f32[128,4]{0,1:T(4,128)S(1)}, f32[128,4]{0,1:T(4,128)}, u32[]{:S(2)}) copy-start(f32[128,4]{0,1:T(4,128)} %get-tuple-element.222) | copy-start | bytes 6148
  283.6 3.8 %copy-start.33 = (f32[8,1,64]{2,0,1:T(8,128)S(1)}, f32[8,1,64]{2,0,1:T(8,128)}, u32[]{:S(2)}) copy-start(f32[8,1,64]{2,0,1:T(8,128)} %copy.299) | copy-start | bytes 6148
  294.0 1.7 copy-start.25
  294.0 1.7 copy-start.26
  294.0 1.7 copy-start.35
  294.0 1.7 copy-start.42
  294.0 1.7 copy-start.44
  294.0 1.7 copy-start.46
  294.3 3.1 copy-start.31
  294.9 3.5 %copy-start.27 = (f32[1,256,64]{2,1,0:T(8,128)S(1)}, f32[1,256,64]{2,1,0:T(8,128)}, u32[]{:S(2)}) copy-start(f32[1,256,64]{2,1,0:T(8,128)} %copy.255) | copy-start | bytes 196612
  295.0 3.5 %copy-start.28 = (f32[1,256,64]{2,1,0:T(8,128)S(1)}, f32[1,256,64]{2,1,0:T(8,128)}, u32[]{:S(2)}) copy-start(f32[1,256,64]{2,1,0:T(8,128)} %copy.254) | copy-start | bytes 196612
  295.0 3.5 %copy-start.34 = (f32[1024,4]{0,1:T(4,128)S(1)}, f32[1024,4]{0,1:T(4,128)}, u32[]{:S(2)}) copy-start(f32[1024,4]{0,1:T(4,128)} %get-tuple-element.230) | copy-start | bytes 49156
  295.0 3.5 %copy-start.56 = (f32[4]{0:T(128)S(1)}, f32[4]{0:T(128)}, u32[]{:S(2)}) copy-start(f32[4]{0:T(128)} %copy-done.55) | copy-start | bytes 52
  295.0 3.5 %copy-start.60 = (f32[4]{0:T(128)S(1)}, f32[4]{0:T(128)}, u32[]{:S(2)}) copy-start(f32[4]{0:T(128)} %copy-done.59) | copy-start | bytes 52
  295.0 3.5 %copy-start.62 = (f32[4]{0:T(128)S(1)}, f32[4]{0:T(128)}, u32[]{:S(2)}) copy-start(f32[4]{0:T(128)} %get-tuple-element.211) | copy-start | bytes 52
  295.0 3.5 %copy-start.65 = (f32[4]{0:T(128)S(1)}, f32[4]{0:T(128)}, u32[]{:S(2)}) copy-start(f32[4]{0:T(128)} %get-tuple-element.122) | copy-start | bytes 52
  297.4 3.6 %copy-start.2 = (f32[4,4,8,8,128]{4,3,2,1,0:T(8,128)S(1)}, f32[4,4,8,8,128]{4,3,2,1,0:T(8,128)}, u32[]{:S(2)}) copy-start(f32[4,4,8,8,128]{4,3,2,1,0:T(8,128)} %fusion.22) | copy-start | bytes 1572868
  297.5 3.6 %copy-start.30 = (f32[512,4]{0,1:T(4,128)S(1)}, f32[512,4]{0,1:T(4,128)}, u32[]{:S(2)}) copy-start(f32[512,4]{0,1:T(4,128)} %get-tuple-element.209) | copy-start | bytes 24580
  298.4 3.3 copy-start.39
  301.1 30.2 %copy-start.1 = (bf16[64,2048]{1,0:T(8,128)(2,1)S(1)}, bf16[64,2048]{1,0:T(8,128)(2,1)}, u32[]{:S(2)}) copy-start(bf16[64,2048]{1,0:T(8,128)(2,1)} %param.18) | copy-start | bytes 786436
  301.1 30.2 %copy-start.29 = (f32[1,1,2048]{2,0,1:T(1,128)S(1)}, f32[1,1,2048]{2,0,1:T(1,128)}, u32[]{:S(2)}) copy-start(f32[1,1,2048]{2,0,1:T(1,128)} %get-tuple-element.170) | copy-start | bytes 24580
  (40 other events, 50.3 us)
Sparse Core Ops, SparseCore 0:
  100.9 76.9 all-gather.10
  181.0 105.9 all-gather.12
where the time goes:
time: 345 us; the launch traced here: 344 us
  blocking collectives  209 us (61%)
  local copies, waits for them, and re-layouts  52.2 us (15%)
  matrix products  26.9 us (8%)
  waiting for transfers between devices  20 us (6%)
  other arithmetic  17 us (5%)
  between operations  14.7 us (4%)
  starting transfers between devices  3.69 us (1%)
    all_gather x4, blocking collectives, collected_together(): both, at, found = (lax.all_gather(jnp.concatenate(lines), axis), 0, {})  90.9 us
    psum x4, blocking collectives, over_axes(): return functools.reduce(lax.psum, axes, shard)  89.4 us
    slice x36, local copies, waits for them, and re-layouts, carried_in(): so_far = combine(so_far, jax.tree.map(lambda part: part[k], pieces))  35.4 us
    all_to_all x1, blocking collectives, per_device(): lax.all_to_all(retained, TP, split_axis=0, concat_axis=1, tiled=True)  28.7 us
    all_to_all x1, waiting for transfers between devices, copy_for_each(): lax.all_to_all(jnp.broadcast_to(shard[None], (devices, *shard.shape)), ax...  19.2 us
  transfers between devices with their start and end apart: 3, of which 1 were waited for; matrix products, arithmetic and copies ran while one was open for 24% of the time, Pallas kernels for 0%

commit v1 on v0

v1 whole, which is shorter than its diff:
```python
import functools

import jax
import jax.numpy as jnp
import numpy as np
from jax import lax
from jax.experimental import pallas as pl
from jax.experimental.pallas import tpu as pltpu
from jax.sharding import Mesh
from jax.sharding import PartitionSpec as P

HEAD = 64
HALF = HEAD // 2
BLOCK = 128
SP = ("sp_0", "sp_1")
TP = ("tp_0", "tp_1")
SP_TP = SP + TP
EPSILON = 1e-06
ROTARY_BASE = 10000.0
F32, BF16 = jnp.float32, jnp.bfloat16
MESH = pl.DeviceIdType.MESH
VMEM_LIMIT = 60 * 1024 * 1024


def remote(src, dst, send_sem, recv_sem, device):
    return pltpu.make_async_remote_copy(
        src_ref=src, dst_ref=dst, send_sem=send_sem, recv_sem=recv_sem,
        device_id=device, device_id_type=MESH,
    )


def place():
    return {a: lax.axis_index(a) for a in SP_TP}


def tp_peers(at, nx):
    core, x = at["tp_1"], at["tp_0"]
    peers = [{"tp_0": x, "tp_1": 1 - core}]
    for k in range(1, nx):
        there = lax.rem(x + k, nx)
        peers += [{"tp_0": there, "tp_1": core}, {"tp_0": there, "tp_1": 1 - core}]
    return peers


def line_peers(at, axis, n):
    return [{axis: lax.rem(at[axis] + k, n)} for k in range(1, n)]


def greet(peers):
    barrier = pltpu.get_barrier_semaphore()
    for peer in peers:
        pl.semaphore_signal(barrier, inc=1, device_id=peer, device_id_type=MESH)
    pl.semaphore_wait(barrier, len(peers))


class Line:
    def __init__(self, at, axis, n, send_sems, recv_sems):
        self.me, self.axis, self.n = at[axis], axis, n
        self.send_sems, self.recv_sems = send_sems, recv_sems
        self.sent = []

    def start(self, source_of, slots):
        for k in range(1, self.n):
            there = lax.rem(self.me + k, self.n)
            copy = remote(
                source_of(there), slots.at[self.me], self.send_sems.at[k],
                self.recv_sems.at[self.me], {self.axis: there},
            )
            copy.start()
            self.sent.append(copy)

    def wait(self, slots):
        for k in range(1, self.n):
            source = lax.rem(self.me + self.n - k, self.n)
            remote(
                slots.at[source], slots.at[source], self.send_sems.at[k],
                self.recv_sems.at[source], {self.axis: source},
            ).wait_recv()

    def drain(self):
        for copy in self.sent:
            copy.wait_send()


class Gather:
    def __init__(self, at, nx, rows, slot, sems):
        self.x, self.core, self.nx, self.rows, self.slot = at["tp_0"], at["tp_1"], nx, rows, slot
        self.send_sems, self.recv_sems = sems
        self.half = rows // 2
        self.sent = []

    def index(self, steps):
        return lax.rem(self.x + self.nx + steps, self.nx)

    def put(self, src, x_of, core_of, first, count, sem, device):
        copy = remote(
            src, self.slot(x_of * 2 + core_of, first, count), self.send_sems.at[sem],
            self.recv_sems.at[sem], device,
        )
        copy.start()
        self.sent.append(copy)

    def came(self, x_of, core_of, first, count, sem):
        view = self.slot(x_of * 2 + core_of, first, count)
        remote(view, view, self.send_sems.at[sem], self.recv_sems.at[sem], {"tp_0": self.x}).wait_recv()

    def start(self, own):
        x, core, h = self.x, self.core, self.half
        right, left = {"tp_0": self.index(1)}, {"tp_0": self.index(-1)}
        self.put(own(0, h), x, core, 0, h, 0, right)
        self.put(own(h, h), x, core, h, h, 2, left)
        self.put(own(h, h), x, core, h, h, 1, right)
        self.put(own(0, h), x, core, 0, h, 3, left)
        self.put(own(0, self.rows), x, core, 0, self.rows, 6, {"tp_1": 1 - core})

    def forward(self):
        core, h = self.core, self.half
        left, right, over = self.index(-1), self.index(1), {"tp_1": 1 - core}
        self.came(left, core, 0, h, 0)
        self.put(self.slot(left * 2 + core, 0, h), left, core, 0, h, 4, {"tp_0": right})
        self.came(right, core, h, h, 2)
        self.put(self.slot(right * 2 + core, h, h), right, core, h, h, 5, {"tp_0": left})
        self.came(left, core, h, h, 1)
        self.put(self.slot(left * 2 + core, 0, self.rows), left, core, 0, self.rows, 7, over)
        self.came(right, core, 0, h, 3)
        self.put(self.slot(right * 2 + core, 0, self.rows), right, core, 0, self.rows, 8, over)

    def finish(self):
        core, h, n = self.core, self.half, self.rows
        far, over = self.index(2), {"tp_1": 1 - core}
        self.came(far, core, 0, h, 4)
        self.came(far, core, h, h, 5)
        self.put(self.slot(far * 2 + core, 0, n), far, core, 0, n, 9, over)
        for sem, steps in ((6, 0), (7, -1), (8, 1), (9, 2)):
            self.came(self.index(steps), 1 - core, 0, n, sem)

    def drain(self):
        for copy in self.sent:
            copy.wait_send()


GATHER_SEMS = 10


def first_kernel(
    sizes, part_ref, lat_ref, w_ref, mod_ref, all_ref, wall_ref,
    ybuf, zbuf, tbuf, ysum, zsum, w_yz, w_zy,
    y_send, y_recv, z_send, z_recv, t_send, t_recv, g_send, g_recv,
    wa_send, wa_recv, wb_send, wb_recv, wc_send, wc_recv, wd_send, wd_recv,
):
    ny, nz, nx = sizes
    at = place()
    y, z, x, core = at["sp_1"], at["sp_0"], at["tp_0"], at["tp_1"]
    t = x * 2 + core
    tps = tp_peers(at, nx)
    greet(line_peers(at, "sp_1", ny) + line_peers(at, "sp_0", nz) + tps)
    along_y = Line(at, "sp_1", ny, y_send, y_recv)
    along_z = Line(at, "sp_0", nz, z_send, z_recv)
    along_y.start(lambda there: part_ref, ybuf)
    rows = lat_ref.shape[0]
    gather = Gather(at, nx, rows, lambda s, a, n: all_ref.at[s, pl.ds(a, n)], (g_send, g_recv))
    gather.start(lambda a, n: lat_ref.at[pl.ds(a, n)])
    depth = w_ref.shape[0]
    lanes = pl.ds(pl.multiple_of(t * 256, 256), 128)
    w_yz[z, y] = w_ref[:, lanes]
    lanes = pl.ds(pl.multiple_of(t * 256 + 128, 128), 128)
    w_zy[y, z] = w_ref[:, lanes]
    all_ref[t] = lat_ref[...]
    ybuf[y] = part_ref[...]
    along_y.wait(ybuf)
    ysum[...] = sum(ybuf[k] for k in range(ny))
    along_z.start(lambda there: ysum, zbuf)
    wa = Line(at, "sp_1", ny, wa_send, wa_recv)
    wa.start(lambda there: w_yz.at[z, y], w_yz.at[z])
    wb = Line(at, "sp_0", nz, wb_send, wb_recv)
    wb.start(lambda there: w_zy.at[y, z], w_zy.at[y])
    zbuf[z] = ysum[...]
    gather.forward()
    along_z.wait(zbuf)
    zsum[...] = sum(zbuf[k] for k in range(nz))
    sent = []
    for k, peer in enumerate(tps):
        copy = remote(zsum, tbuf.at[t], t_send.at[k], t_recv.at[t], peer)
        copy.start()
        sent.append(copy)
    tbuf[t] = zsum[...]
    gather.finish()
    wa.wait(w_yz.at[z])
    wc = Line(at, "sp_0", nz, wc_send, wc_recv)
    wc.start(lambda there: w_yz.at[z], w_yz)
    wb.wait(w_zy.at[y])
    wd = Line(at, "sp_1", ny, wd_send, wd_recv)
    wd.start(lambda there: w_zy.at[y], w_zy)
    for k, peer in enumerate(tps):
        s = peer.get("tp_0", x) * 2 + peer["tp_1"]
        remote(tbuf.at[s], tbuf.at[s], t_send.at[k], t_recv.at[s], peer).wait_recv()
    for s in range(2 * nx):
        mod_ref[:, s * 256 : (s + 1) * 256] = tbuf[s]
    wc.wait(w_yz)
    wd.wait(w_zy)
    for a in range(nz):
        for b in range(ny):
            first = (a * ny + b) * depth
            wall_ref[first : first + depth, 0:128] = w_yz[a, b]
            wall_ref[first : first + depth, 128:256] = w_zy[b, a]
    for line in (along_y, along_z, wa, wb, wc, wd, gather):
        line.drain()
    for copy in sent:
        copy.wait_send()


def head_masks(heads):
    lane = lax.broadcasted_iota(jnp.int32, (1, heads * HEAD), 1)
    return [(lane >= h * HEAD) & (lane < (h + 1) * HEAD) for h in range(heads)]


def squeezed(full, masks):
    return sum(
        jnp.where(m, full[h * HEAD : (h + 1) * HEAD], 0.0) for h, m in enumerate(masks)
    )


def spread_out(packed, masks):
    return jnp.concatenate([jnp.where(m, packed, 0.0) for m in masks], axis=0)


def rotated(u, cos, sin, low):
    width = u.shape[1]
    partner = jnp.where(low, pltpu.roll(u, width - HALF, 1), pltpu.roll(u, HALF, 1))
    return u * cos + partner * sin


def outer(keys, values):
    return lax.dot_general(
        keys.astype(BF16), values, (((0,), (0,)), ((), ())), preferred_element_type=F32
    )


def project_kernel(
    sizes, ctx_len, all_ref, ctx_ref, mod_ref, gain_ref, wq_ref, wk_ref, wv_ref,
    cos_ref, sin_ref, base_ref, ld_ref,
    q_ref, k_ref, v_ref, u_ref, st_ref, normed,
):
    ny, nz, nx = sizes
    tokens, width = q_ref.shape
    heads = width // HEAD
    ctx_rows = ctx_ref.shape[0]
    gain = gain_ref[...]

    def norm(rows, c):
        wide = rows.astype(F32)
        r = lax.rsqrt(jnp.mean(wide * wide, axis=-1, keepdims=True) + EPSILON)
        scale = gain * (1.0 + mod_ref[3 * c + 1 : 3 * c + 2])
        return (wide * r * scale + mod_ref[3 * c : 3 * c + 1]).astype(BF16)

    @pl.loop(0, tokens // 64)
    def _(i):
        rows = pl.ds(pl.multiple_of(i * 64, 64), 64)
        normed[rows] = norm(all_ref[rows], 0)

    normed[tokens : tokens + ctx_rows] = norm(ctx_ref[...], 1)
    lane = lax.broadcasted_iota(jnp.int32, (1, width), 1)
    low = lax.rem(lane, HEAD) < HALF
    sign = jnp.where(low, -1.0, 1.0)
    cos_off, sin_off = cos_ref[...], sin_ref[...]
    cos = base_ref[0:1] * cos_off - base_ref[1:2] * sin_off
    sin = (base_ref[1:2] * cos_off + base_ref[0:1] * sin_off) * sign
    ccos = base_ref[2:3] * cos_off[:ctx_rows] - base_ref[3:4] * sin_off[:ctx_rows]
    csin = (base_ref[3:4] * cos_off[:ctx_rows] + base_ref[2:3] * sin_off[:ctx_rows]) * sign
    both = normed[...]
    k_all = jnp.dot(both, wk_ref[...], preferred_element_type=F32)
    v_all = jnp.dot(both, wv_ref[...], preferred_element_type=F32).astype(BF16)
    v_ref[...] = v_all[:tokens]
    k_ref[...] = rotated(k_all[:tokens], cos, sin, low).astype(BF16)
    ck = rotated(k_all[tokens:], ccos, csin, low).astype(BF16).astype(F32)
    cv = v_all[tokens:]
    masks = head_masks(heads)
    ldf, ldb = ld_ref[0:1], ld_ref[1:2]
    sp = lax.axis_index("sp_0") * ny + lax.axis_index("sp_1")
    spot = (sp * ctx_rows + lax.broadcasted_iota(jnp.int32, (ctx_rows, 1), 0)).astype(F32)
    cf = squeezed(outer(ck * jnp.exp(ldf * (ctx_len - 1.0 - spot)), cv), masks)
    cb = squeezed(outer(ck * jnp.exp(ldb * spot), cv), masks)
    at = lax.broadcasted_iota(jnp.int32, (BLOCK, 1), 0).astype(F32)
    to_end, to_start = jnp.exp(ldf * (BLOCK - 1.0 - at)), jnp.exp(ldb * at)
    blocks = tokens // BLOCK
    gf, gb = jnp.exp(ldf * BLOCK), jnp.exp(ldb * BLOCK)
    sf = jnp.zeros((HEAD, width), F32)
    ub = []
    for b in range(blocks):
        keys = k_ref[b * BLOCK : (b + 1) * BLOCK].astype(F32)
        values = v_ref[b * BLOCK : (b + 1) * BLOCK]
        u_ref[b] = sf
        sf = gf * sf + squeezed(outer(keys * to_end, values), masks)
        ub.append(squeezed(outer(keys * to_start, values), masks))
    sb = jnp.zeros((HEAD, width), F32)
    for b in reversed(range(blocks)):
        u_ref[blocks + b] = sb
        sb = gb * sb + ub[b]
    part = HEAD // ny
    for s in range(ny):
        rows = slice(s * part, (s + 1) * part)
        st_ref[s] = jnp.concatenate([sf[rows], sb[rows], cf[rows], cb[rows]], axis=0).astype(BF16)
    q_all = jnp.dot(both[:tokens], wq_ref[...], preferred_element_type=F32)
    q_ref[...] = (rotated(q_all, cos, sin, low) * HEAD ** (-0.5)).astype(BF16)


def state_kernel(
    sizes, tokens, st_ref, ld_ref, ent_ref, r1, s2, r2, s3,
    a_send, a_recv, b_send, b_recv, c_send, c_recv,
):
    ny, nz, nx = sizes
    at = place()
    y, z = at["sp_1"], at["sp_0"]
    greet(line_peers(at, "sp_1", ny) + line_peers(at, "sp_0", nz))
    part = HEAD // ny
    one = Line(at, "sp_1", ny, a_send, a_recv)
    one.start(lambda there: st_ref.at[there], r1)
    ldf, ldb = ld_ref[0:1], ld_ref[1:2]
    r1[y] = st_ref[y]
    one.wait(r1)
    got = [r1[j].astype(F32) for j in range(ny)]
    gf, gb = jnp.exp(ldf * tokens), jnp.exp(ldb * tokens)
    ahead = [jnp.zeros_like(got[0][:part])]
    for j in range(ny):
        ahead.append(gf * ahead[-1] + got[j][:part])
    total_f = ahead.pop()
    behind = [jnp.zeros_like(ahead[0])]
    for j in reversed(range(ny)):
        behind.append(gb * behind[-1] + got[j][part : 2 * part])
    total_b = behind.pop()
    behind = behind[::-1]
    ctx = sum(got)
    ctx_f, ctx_b = ctx[2 * part : 3 * part], ctx[3 * part :]
    row = float(tokens * ny)
    for k in range(nz):
        there = lax.rem(z + k, nz)
        gap = (there - z).astype(F32)
        to_f = jnp.where(there > z, 1.0, 0.0) * jnp.exp(ldf * (row * jnp.maximum(gap - 1.0, 0.0)))
        to_b = jnp.where(there < z, 1.0, 0.0) * jnp.exp(ldb * (row * jnp.maximum(-gap - 1.0, 0.0)))
        start_f = jnp.exp(ldf * (row * there.astype(F32)))
        start_b = jnp.exp(ldb * (row * (nz - 1 - there).astype(F32)))
        s2[there] = jnp.concatenate(
            [to_f * total_f + start_f * ctx_f, to_b * total_b + start_b * ctx_b], axis=0
        ).astype(BF16)
    r2[z] = s2[z]
    two = Line(at, "sp_0", nz, b_send, b_recv)
    two.start(lambda there: s2.at[there], r2)
    two.wait(r2)
    entering = sum(r2[j].astype(F32) for j in range(nz))
    for j in range(ny):
        s3[j] = jnp.concatenate(
            [
                ahead[j] + jnp.exp(ldf * float(tokens * j)) * entering[:part],
                behind[j] + jnp.exp(ldb * float(tokens * (ny - 1 - j))) * entering[part:],
            ],
            axis=0,
        ).astype(BF16)
    three = Line(at, "sp_1", ny, c_send, c_recv)
    three.start(lambda there: s3.at[there], ent_ref)
    ent_ref[y] = s3[y]
    three.wait(ent_ref)
    for line in (one, two, three):
        line.drain()


def averaged(values, average):
    high = values.astype(BF16)
    rest = (values - high.astype(F32)).astype(BF16)
    return jnp.dot(high, average, preferred_element_type=F32) + jnp.dot(
        rest, average, preferred_element_type=F32
    )


def retain_kernel(sizes, q_ref, k_ref, v_ref, u_ref, ent_ref, ld_ref, hg_ref, out_ref, decay):
    ny, nz, nx = sizes
    tokens, width = q_ref.shape
    heads = width // HEAD
    blocks = tokens // BLOCK
    part = HEAD // ny
    masks = head_masks(heads)
    ldf, ldb = ld_ref[0:1], ld_ref[1:2]
    row = lax.broadcasted_iota(jnp.int32, (BLOCK, BLOCK), 0)
    col = lax.broadcasted_iota(jnp.int32, (BLOCK, BLOCK), 1)
    gap = (row - col).astype(F32)
    for h in range(heads):
        f, b = ldf[:, h * HEAD : h * HEAD + 1], ldb[:, h * HEAD : h * HEAD + 1]
        decay[h * BLOCK : (h + 1) * BLOCK] = jnp.where(
            gap >= 0, jnp.exp(f * jnp.maximum(gap, 0.0)), 0.0
        ) + jnp.where(gap <= 0, jnp.exp(b * jnp.maximum(-gap, 0.0)), 0.0)
    ent = [ent_ref[s].astype(F32) for s in range(ny)]
    enter_f = jnp.concatenate([e[:part] for e in ent], axis=0)
    enter_b = jnp.concatenate([e[part:] for e in ent], axis=0)
    at = lax.broadcasted_iota(jnp.int32, (BLOCK, 1), 0).astype(F32)
    read_f, read_b = jnp.exp(ldf * (at + 1.0)), jnp.exp(ldb * (BLOCK - at))
    a = lax.broadcasted_iota(jnp.int32, (width, width), 0)
    b = lax.broadcasted_iota(jnp.int32, (width, width), 1)
    average = jnp.where(a // HEAD == b // HEAD, 1.0 / HEAD, 0.0).astype(BF16)
    for i in range(blocks):
        rows = slice(i * BLOCK, (i + 1) * BLOCK)
        q = q_ref[rows]
        wide = q.astype(F32)
        stacked = jnp.concatenate([jnp.where(m, wide, 0.0) for m in masks], axis=0).astype(BF16)
        scores = lax.dot_general(
            stacked, k_ref[rows], (((1,), (1,)), ((), ())), preferred_element_type=F32
        )
        weights = (scores * decay[...]).astype(BF16)
        inside = jnp.dot(weights, v_ref[rows], preferred_element_type=F32)
        state_f = u_ref[i] + jnp.exp(ldf * float(BLOCK * i)) * enter_f
        state_b = u_ref[blocks + i] + jnp.exp(ldb * float(BLOCK * (blocks - 1 - i))) * enter_b
        states = jnp.concatenate(
            [spread_out(state_f, masks), spread_out(state_b, masks)], axis=0
        ).astype(BF16)
        readers = jnp.concatenate([wide * read_f, wide * read_b], axis=1).astype(BF16)
        o = jnp.dot(readers, states, preferred_element_type=F32)
        for h, m in enumerate(masks):
            o = o + jnp.where(m, inside[h * BLOCK : (h + 1) * BLOCK], 0.0)
        centred = o - averaged(o, average)
        spread = averaged(centred * centred, average)
        out_ref[rows] = (centred * lax.rsqrt(spread + EPSILON) * hg_ref[...]).astype(BF16)


def output_kernel(
    sizes, ret_ref, wall_ref, all_ref, mod_ref, out_ref, gathered, done, landed,
    g_send, g_recv, o_send, o_recv,
):
    ny, nz, nx = sizes
    at = place()
    x, core = at["tp_0"], at["tp_1"]
    t = x * 2 + core
    tps = tp_peers(at, nx)
    greet(tps)
    tokens, width = ret_ref.shape
    own_rows = out_ref.shape[0]
    chunk = 2 * own_rows
    chunks = tokens // chunk
    gathers = []
    for c in range(chunks):
        g = Gather(
            at, nx, chunk, lambda s, a, n, c=c: gathered.at[s, pl.ds(c * chunk + a, n)],
            (g_send.at[c], g_recv.at[c]),
        )
        g.start(lambda a, n, c=c: ret_ref.at[pl.ds(c * chunk + a, n)])
        gathers.append(g)
    gathered[t] = ret_ref[...]
    gate_row = mod_ref[2:3, pl.ds(pl.multiple_of(t * width, width), width)]
    sent = []
    for g in gathers:
        g.forward()
    for c, g in enumerate(gathers):
        g.finish()
        rows = slice(c * chunk, (c + 1) * chunk)
        mixed = sum(
            jnp.dot(
                gathered[s, rows], wall_ref[s * width : (s + 1) * width],
                preferred_element_type=F32,
            )
            for s in range(2 * nx)
        )
        lat = all_ref[rows, pl.ds(pl.multiple_of(t * width, width), width)].astype(F32)
        result = (lat + gate_row * mixed).astype(BF16)
        done[2 * c] = result[:own_rows]
        done[2 * c + 1] = result[own_rows:]
        for k in range(2):
            owner = 2 * c + k
            copy = remote(
                done.at[owner], landed.at[t], o_send.at[owner], o_recv.at[t],
                {"tp_0": jnp.int32(c), "tp_1": jnp.int32(k)},
            )
            mine = owner == t

            @pl.when(jnp.logical_not(mine))
            def _(copy=copy):
                copy.start()

            sent.append((mine, copy))
    landed[t] = done[t]
    for k, peer in enumerate(tps):
        s = peer.get("tp_0", x) * 2 + peer["tp_1"]
        remote(landed.at[s], landed.at[s], o_send.at[0], o_recv.at[s], peer).wait_recv()
    for s in range(2 * nx):
        out_ref[:, s * width : (s + 1) * width] = landed[s]
    for g in gathers:
        g.drain()
    for mine, copy in sent:

        @pl.when(jnp.logical_not(mine))
        def _(copy=copy):
            copy.wait_send()


def call(kernel, outs, scratch, collective, ins):
    spec = pl.BlockSpec(memory_space=pltpu.VMEM)
    more = {} if collective is None else {"collective_id": collective, "has_side_effects": True}
    return pl.pallas_call(
        kernel,
        out_shape=outs,
        in_specs=[spec] * len(ins),
        out_specs=jax.tree.map(lambda _: spec, outs),
        scratch_shapes=scratch,
        compiler_params=pltpu.CompilerParams(vmem_limit_bytes=VMEM_LIMIT, **more),
    )(*ins)


def turns(positions):
    frequency = ROTARY_BASE ** -np.linspace(0.0, 1.0, HALF)
    angles = np.asarray(positions, np.float64)[:, None] * frequency[None]
    return np.cos(angles), np.sin(angles)


def per_device(
    sizes, latent, context, condition, context_condition, modulation_weight, norm_gain,
    query_weight, key_weight, value_weight, log_decay, head_gain, output_weight,
):
    ny, nz, nx = sizes
    nt = 2 * nx
    d = latent.shape[1]
    width = query_weight.shape[1]
    heads = width // HEAD
    own = latent.shape[0]
    tokens = own * nt
    ctx_rows = context.shape[0]
    ctx_len = ctx_rows * ny * nz
    seq = lax.axis_index(SP)
    dma = pltpu.SemaphoreType.DMA
    activated = jax.nn.silu(jnp.stack([condition, context_condition])).astype(BF16)
    depth, _, cols = modulation_weight.shape
    mine = lax.dynamic_slice_in_dim(activated, seq * depth, depth, 1)
    part = jnp.dot(
        mine, modulation_weight.reshape(depth, 3 * cols), preferred_element_type=F32
    ).reshape(6, cols)
    part = jnp.pad(part, ((0, 2), (0, 0)))
    wrows = output_weight.shape[0]
    modulation, rows, wall = call(
        functools.partial(first_kernel, sizes),
        [
            jax.ShapeDtypeStruct((8, d), F32),
            jax.ShapeDtypeStruct((nt, own, d), BF16),
            jax.ShapeDtypeStruct((output_weight.shape[0] * ny * nz, cols), BF16),
        ],
        [
            pltpu.VMEM((ny, 8, cols), F32), pltpu.VMEM((nz, 8, cols), F32),
            pltpu.VMEM((nt, 8, cols), F32), pltpu.VMEM((8, cols), F32), pltpu.VMEM((8, cols), F32),
            pltpu.VMEM((nz, ny, wrows, 128), BF16), pltpu.VMEM((ny, nz, wrows, 128), BF16),
            dma((ny,)), dma((ny,)), dma((nz,)), dma((nz,)), dma((nt,)), dma((nt,)),
            dma((GATHER_SEMS,)), dma((GATHER_SEMS,)),
            dma((ny,)), dma((ny,)), dma((nz,)), dma((nz,)),
            dma((nz,)), dma((nz,)), dma((ny,)), dma((ny,)),
        ],
        0,
        [part, latent, output_weight],
    )
    rows = rows.reshape(tokens, d)
    tile = lambda a: np.tile(np.asarray(a, np.float32), (1, heads * 2))
    cos_off, sin_off = (jnp.asarray(tile(a)) for a in turns(np.arange(tokens)))
    bases = np.stack(
        [tile(a) for a in turns(ctx_len + tokens * np.arange(ny * nz))]
        + [tile(a) for a in turns(ctx_rows * np.arange(ny * nz))],
        axis=1,
    )
    base = lax.dynamic_index_in_dim(jnp.asarray(bases), seq, 0, keepdims=False)
    rates = jnp.repeat(log_decay, HEAD, axis=1)
    blocks = tokens // BLOCK
    part_rows = HEAD // ny
    q, k, v, u, st = call(
        functools.partial(project_kernel, sizes, ctx_len),
        [
            jax.ShapeDtypeStruct((tokens, width), BF16),
            jax.ShapeDtypeStruct((tokens, width), BF16),
            jax.ShapeDtypeStruct((tokens, width), BF16),
            jax.ShapeDtypeStruct((2 * blocks, HEAD, width), F32),
            jax.ShapeDtypeStruct((ny, 4 * part_rows, width), BF16),
        ],
        [pltpu.VMEM((tokens + ctx_rows, d), BF16)],
        None,
        [
            rows, context, modulation, norm_gain.reshape(1, d), query_weight, key_weight,
            value_weight, cos_off, sin_off, base, rates,
        ],
    )
    entering = call(
        functools.partial(state_kernel, sizes, tokens),
        jax.ShapeDtypeStruct((ny, 2 * part_rows, width), BF16),
        [
            pltpu.VMEM((ny, 4 * part_rows, width), BF16),
            pltpu.VMEM((nz, 2 * part_rows, width), BF16),
            pltpu.VMEM((nz, 2 * part_rows, width), BF16),
            pltpu.VMEM((ny, 2 * part_rows, width), BF16),
            dma((ny,)), dma((ny,)), dma((nz,)), dma((nz,)), dma((ny,)), dma((ny,)),
        ],
        1,
        [st, rates],
    )
    retained = call(
        functools.partial(retain_kernel, sizes),
        jax.ShapeDtypeStruct((tokens, width), BF16),
        [pltpu.VMEM((heads * BLOCK, BLOCK), F32)],
        None,
        [q, k, v, u, entering, rates, head_gain.reshape(1, width)],
    )
    chunks = tokens // (2 * own)
    return call(
        functools.partial(output_kernel, sizes),
        jax.ShapeDtypeStruct((own, d), BF16),
        [
            pltpu.VMEM((nt, tokens, width), BF16),
            pltpu.VMEM((nt, own, width), BF16),
            pltpu.VMEM((nt, own, width), BF16),
            dma((chunks, GATHER_SEMS)), dma((chunks, GATHER_SEMS)), dma((nt,)), dma((nt,)),
        ],
        2,
        [retained, wall, rows, modulation],
    )


def solution(mesh, ny=8, nz=8, nx=4):
    split = Mesh(mesh.devices.reshape(nz, ny, nx, 2), SP_TP)
    placed = (
        P(SP_TP, None), P(SP, None), P(), P(), P(SP, None, TP), P(), P(None, TP), P(None, TP),
        P(None, TP), P(None, TP), P(TP), P(SP, None),
    )
    return jax.shard_map(
        functools.partial(per_device, (ny, nz, nx)), mesh=split, in_specs=placed,
        out_specs=P(SP_TP, None), check_vma=False,
    )
```

time: 345 us -> 111 us (0.32)
  the two profiles are of different devices: /device:TPU:1 before, /device:TPU:7 now
where the time goes in v1:
time: 111 us
  Pallas kernels  104 us (94%)
  local copies, waits for them, and re-layouts  5.78 us (5%)
    pallas_call x5, Pallas kernels, call(): pl.pallas_call(kernel, out_shape=outs, in_specs=[spec] * len(ins), out_sp...  104 us

profile of v1, /device:TPU:7, one launch (start us, length us, event | category | flops | bytes accessed | tf_op | source)
XLA Modules:
  0.0 111.0 jit_solution(3134899122105670294)
XLA Ops:
  0.0 1.3 %dynamic-slice_bitcast_fusion.base_ref = f32[4,256]{1,0:T(4,128)} fusion(f32[64,4,256]{2,1,0:T(4,128)} %constant.35.clone, s32[]{:T(128)S(6)} %select_n.8), kind=kLoop, calls=%fused_computation.2 | loop fusion | bytes 8196 | tf_op jit(solution)/shard_map/jit(dynamic_index_in_dim)/squeeze | solution.py:560
  1.3 0.7 broadcast_in_dim.3
  2.0 0.7 reshape.22.ld_ref
  2.7 0.8 copy.17
  3.5 0.9 fusion.2
  4.4 0.6 pad.4.part_ref
  5.0 43.5 %shard_map.145 = (f32[8,2048]{1,0:T(8,128)}, bf16[8,64,2048]{2,1,0:T(8,128)(2,1)}, bf16[2048,256]{1,0:T(8,128)(2,1)}) custom-call(f32[8,256]{1,0:T(8,128)} %pad.4.part_ref, bf16[64,2048]{1,0:T(8,128)(2,1)} %lat_ref.1, bf16[32,2048]{1,0:T(8,128)(2,1)} %w_ref.1), custom_call_target="tpu_custom_call" | custom-call | tf_op jit(solution)/shard_map/pallas_call | solution.py:494
  48.5 8.8 %shard_map.146 = (bf16[512,256]{1,0:T(8,128)(2,1)}, bf16[512,256]{1,0:T(8,128)(2,1)}, bf16[512,256]{1,0:T(8,128)(2,1)}, f32[8,64,256]{2,1,0:T(8,128)}, bf16[8,32,256]{2,1,0:T(8,128)(2,1)}) custom-call(bf16[512,2048]{1,0:T(8,128)(2,1)} %bitcast.10, bf16[16,2048]{1,0:T(8,128)(2,1)} %ctx_ref.1, f32[8,2048]{1,0:T(8,128)} %get-tuple-element.14.mod_ref, ...), custom_call_target="tpu_custom_call" | custom-call | tf_op jit(solution)/shard_map/pallas_call | solution.py:494
  57.3 19.9 %shard_map.147.ent_ref = bf16[8,16,256]{2,1,0:T(8,128)(2,1)} custom-call(bf16[8,32,256]{2,1,0:T(8,128)(2,1)} %get-tuple-element.19.st_ref, f32[2,256]{1,0:T(2,128)} %reshape.22.ld_ref), custom_call_target="tpu_custom_call" | custom-call | tf_op jit(solution)/shard_map/pallas_call | solution.py:494
  77.2 4.2 %shard_map.148.ret_ref = bf16[512,256]{1,0:T(8,128)(2,1)} custom-call(bf16[512,256]{1,0:T(8,128)(2,1)} %get-tuple-element.15.q_ref, bf16[512,256]{1,0:T(8,128)(2,1)} %get-tuple-element.16.k_ref, bf16[512,256]{1,0:T(8,128)(2,1)} %get-tuple-element.17.v_ref, f32[8,64,256]{2,1,0:T(8,128)} %get-tuple-element.18.u_ref, bf16[8,16,256]{2,1,0:T(8,128)(2,1)} %shard_map.147.ent_ref, ...), custom_call_target="tpu_custom_call" | custom-call | tf_op jit(solution)/shard_map/pallas_call | solution.py:494
  81.5 27.8 %shard_map.149 = bf16[64,2048]{1,0:T(8,128)(2,1)} custom-call(bf16[512,256]{1,0:T(8,128)(2,1)} %shard_map.148.ret_ref, bf16[2048,256]{1,0:T(8,128)(2,1)} %get-tuple-element.20.wall_ref, bf16[512,2048]{1,0:T(8,128)(2,1)} %bitcast.11, f32[8,2048]{1,0:T(8,128)} %get-tuple-element.14.mod_ref), custom_call_target="tpu_custom_call" | custom-call | tf_op jit(solution)/shard_map/pallas_call | solution.py:494
  109.3 1.7 %copy.19 = bf16[64,2048]{1,0:T(8,128)(2,1)} copy(bf16[64,2048]{1,0:T(8,128)(2,1)} %shard_map.149) | data formatting | bytes 524288
  (1 shorter events, 0.0 us)

commit v2 on v1

v2 whole, which is shorter than its diff:
```python
import functools

import jax
import jax.numpy as jnp
import numpy as np
from jax import lax
from jax.experimental import pallas as pl
from jax.experimental.pallas import tpu as pltpu
from jax.sharding import Mesh
from jax.sharding import PartitionSpec as P

HEAD = 64
HALF = HEAD // 2
BLOCK = 128
SP = ("sp_0", "sp_1")
TP = ("tp_0", "tp_1")
SP_TP = SP + TP
EPSILON = 1e-06
ROTARY_BASE = 10000.0
F32, BF16 = jnp.float32, jnp.bfloat16
MESH = pl.DeviceIdType.MESH
VMEM_LIMIT = 60 * 1024 * 1024


def remote(src, dst, send_sem, recv_sem, device):
    return pltpu.make_async_remote_copy(
        src_ref=src, dst_ref=dst, send_sem=send_sem, recv_sem=recv_sem,
        device_id=device, device_id_type=MESH,
    )


def place():
    return {a: lax.axis_index(a) for a in SP_TP}


def tp_peers(at, nx):
    core, x = at["tp_1"], at["tp_0"]
    peers = [{"tp_0": x, "tp_1": 1 - core}]
    for k in range(1, nx):
        there = lax.rem(x + k, nx)
        peers += [{"tp_0": there, "tp_1": core}, {"tp_0": there, "tp_1": 1 - core}]
    return peers


def line_peers(at, axis, n):
    return [{axis: lax.rem(at[axis] + k, n)} for k in range(1, n)]


def greet(peers):
    barrier = pltpu.get_barrier_semaphore()
    for peer in peers:
        pl.semaphore_signal(barrier, inc=1, device_id=peer, device_id_type=MESH)
    return lambda: pl.semaphore_wait(barrier, len(peers))


class Line:
    def __init__(self, at, axis, n, send_sems, recv_sems):
        self.me, self.axis, self.n = at[axis], axis, n
        self.send_sems, self.recv_sems = send_sems, recv_sems
        self.sent = []

    def start(self, source_of, slots):
        for k in range(1, self.n):
            there = lax.rem(self.me + k, self.n)
            copy = remote(
                source_of(there), slots.at[self.me], self.send_sems.at[k],
                self.recv_sems.at[self.me], {self.axis: there},
            )
            copy.start()
            self.sent.append(copy)

    def wait(self, slots):
        for k in range(1, self.n):
            source = lax.rem(self.me + self.n - k, self.n)
            remote(
                slots.at[source], slots.at[source], self.send_sems.at[k],
                self.recv_sems.at[source], {self.axis: source},
            ).wait_recv()

    def drain(self):
        for copy in self.sent:
            copy.wait_send()


class Gather:
    def __init__(self, at, nx, rows, slot, sems):
        self.x, self.core, self.nx, self.rows, self.slot = at["tp_0"], at["tp_1"], nx, rows, slot
        self.send_sems, self.recv_sems = sems
        self.half = rows // 2
        self.sent = []

    def index(self, steps):
        return lax.rem(self.x + self.nx + steps, self.nx)

    def put(self, src, x_of, core_of, first, count, sem, device):
        copy = remote(
            src, self.slot(x_of * 2 + core_of, first, count), self.send_sems.at[sem],
            self.recv_sems.at[sem], device,
        )
        copy.start()
        self.sent.append(copy)

    def came(self, x_of, core_of, first, count, sem):
        view = self.slot(x_of * 2 + core_of, first, count)
        remote(view, view, self.send_sems.at[sem], self.recv_sems.at[sem], {"tp_0": self.x}).wait_recv()

    def start(self, own):
        x, core, h = self.x, self.core, self.half
        right, left = {"tp_0": self.index(1)}, {"tp_0": self.index(-1)}
        self.put(own(0, h), x, core, 0, h, 0, right)
        self.put(own(h, h), x, core, h, h, 2, left)
        self.put(own(h, h), x, core, h, h, 1, right)
        self.put(own(0, h), x, core, 0, h, 3, left)
        self.put(own(0, self.rows), x, core, 0, self.rows, 6, {"tp_1": 1 - core})

    def forward(self):
        core, h = self.core, self.half
        left, right, over = self.index(-1), self.index(1), {"tp_1": 1 - core}
        self.came(left, core, 0, h, 0)
        self.put(self.slot(left * 2 + core, 0, h), left, core, 0, h, 4, {"tp_0": right})
        self.came(right, core, h, h, 2)
        self.put(self.slot(right * 2 + core, h, h), right, core, h, h, 5, {"tp_0": left})
        self.came(left, core, h, h, 1)
        self.put(self.slot(left * 2 + core, 0, self.rows), left, core, 0, self.rows, 7, over)
        self.came(right, core, 0, h, 3)
        self.put(self.slot(right * 2 + core, 0, self.rows), right, core, 0, self.rows, 8, over)

    def finish(self):
        core, h, n = self.core, self.half, self.rows
        far, over = self.index(2), {"tp_1": 1 - core}
        self.came(far, core, 0, h, 4)
        self.came(far, core, h, h, 5)
        self.put(self.slot(far * 2 + core, 0, n), far, core, 0, n, 9, over)
        for sem, steps in ((6, 0), (7, -1), (8, 1), (9, 2)):
            self.came(self.index(steps), 1 - core, 0, n, sem)

    def drain(self):
        for copy in self.sent:
            copy.wait_send()


GATHER_SEMS = 10


def head_masks(heads):
    lane = lax.broadcasted_iota(jnp.int32, (1, heads * HEAD), 1)
    return [(lane >= h * HEAD) & (lane < (h + 1) * HEAD) for h in range(heads)]


def squeezed(full, masks):
    return sum(
        jnp.where(m, full[h * HEAD : (h + 1) * HEAD], 0.0) for h, m in enumerate(masks)
    )


def spread_out(packed, masks):
    return jnp.concatenate([jnp.where(m, packed, 0.0) for m in masks], axis=0)


def rotated(u, cos, sin, low):
    width = u.shape[1]
    partner = jnp.where(low, pltpu.roll(u, width - HALF, 1), pltpu.roll(u, HALF, 1))
    return u * cos + partner * sin


def outer(keys, values):
    return lax.dot_general(
        keys.astype(BF16), values, (((0,), (0,)), ((), ())), preferred_element_type=F32
    )


def averaged(values, average):
    high = values.astype(BF16)
    rest = (values - high.astype(F32)).astype(BF16)
    return jnp.dot(high, average, preferred_element_type=F32) + jnp.dot(
        rest, average, preferred_element_type=F32
    )


def whole_kernel(
    sizes, ctx_len, cond_ref, mw_ref, lat_ref, ctx_ref, w_ref, gain_ref, ld_ref, hg_ref,
    cos_ref, sin_ref, base_ref, wq_hbm, wk_hbm, wv_hbm, out_ref,
    wq, wk, wv, part_s, mod, rows_all, stat, normed, cos_s, sin_s, decay,
    ybuf, zbuf, tbuf, ysum, zsum, w_yz, w_zy, wall,
    k_s, v_s, u_s, o_s, readers, st, r1, s2, r2, s3, ent, ret, gathered, done, landed,
    wt_sem, y_send, y_recv, z_send, z_recv, t_send, t_recv, l_send, l_recv,
    wa_send, wa_recv, wb_send, wb_recv, wc_send, wc_recv, wd_send, wd_recv,
    a_send, a_recv, b_send, b_recv, c_send, c_recv, g_send, g_recv, o_send, o_recv,
):
    ny, nz, nx = sizes
    nt = 2 * nx
    own, d = lat_ref.shape
    tokens = own * nt
    width = hg_ref.shape[1]
    heads = width // HEAD
    blocks = tokens // BLOCK
    part = HEAD // ny
    ctx_rows = ctx_ref.shape[0]
    at = place()
    y, z, x, core = at["sp_1"], at["sp_0"], at["tp_0"], at["tp_1"]
    t, sp = x * 2 + core, z * ny + y
    tps = tp_peers(at, nx)
    weights = [
        pltpu.make_async_copy(a, b, wt_sem.at[i])
        for i, (a, b) in enumerate(((wk_hbm, wk), (wv_hbm, wv), (wq_hbm, wq)))
    ]
    for copy in weights:
        copy.start()
    met = greet(line_peers(at, "sp_1", ny) + line_peers(at, "sp_0", nz) + tps)

    c = cond_ref[...]
    activated = (c / (1.0 + jnp.exp(-c))).astype(BF16)
    depth, _, cols = mw_ref.shape
    entry = lax.broadcasted_iota(jnp.int32, (d, depth), 0)
    place_of = lax.broadcasted_iota(jnp.int32, (d, depth), 1) + sp * depth
    mine = jnp.dot(
        activated, jnp.where(entry == place_of, 1.0, 0.0).astype(BF16), preferred_element_type=F32
    ).astype(BF16)
    parts = [jnp.dot(mine, mw_ref[:, r, :], preferred_element_type=F32) for r in range(3)]
    part_s[...] = jnp.concatenate(
        [parts[r][k : k + 1] for k in range(2) for r in range(3)] + [parts[0][2:4]], axis=0
    )
    met()
    along_y = Line(at, "sp_1", ny, y_send, y_recv)
    along_z = Line(at, "sp_0", nz, z_send, z_recv)
    along_y.start(lambda there: part_s, ybuf)
    spread_rows = Gather(
        at, nx, own, lambda s, a, n: rows_all.at[pl.ds(s * own + a, n)], (l_send, l_recv)
    )
    spread_rows.start(lambda a, n: lat_ref.at[pl.ds(a, n)])
    ybuf[y] = part_s[...]
    rows_all[pl.ds(pl.multiple_of(t * own, own), own)] = lat_ref[...]
    wrows = w_ref.shape[0]
    w_yz[z, y] = w_ref[:, pl.ds(pl.multiple_of(t * 256, 256), 128)]
    w_zy[y, z] = w_ref[:, pl.ds(pl.multiple_of(t * 256 + 128, 128), 128)]
    wa = Line(at, "sp_1", ny, wa_send, wa_recv)
    wa.start(lambda there: w_yz.at[z, y], w_yz.at[z])

    lane = lax.broadcasted_iota(jnp.int32, (1, width), 1)
    low = lax.rem(lane, HEAD) < HALF
    sign = jnp.where(low, -1.0, 1.0)
    repeat = lambda a: jnp.concatenate([a] * (width // a.shape[1]), axis=1)
    base = repeat(base_ref[sp])
    cos_off, sin_off = repeat(cos_ref[...]), repeat(sin_ref[...])
    cos_s[...] = base[0:1] * cos_off - base[1:2] * sin_off
    sin_s[...] = (base[1:2] * cos_off + base[0:1] * sin_off) * sign
    ccos = base[2:3] * cos_off[:ctx_rows] - base[3:4] * sin_off[:ctx_rows]
    csin = (base[3:4] * cos_off[:ctx_rows] + base[2:3] * sin_off[:ctx_rows]) * sign
    masks = head_masks(heads)
    rates = sum(jnp.where(m, ld_ref[:, h : h + 1], 0.0) for h, m in enumerate(masks))
    ldf, ldb = rates[0:1], rates[1:2]
    row = lax.broadcasted_iota(jnp.int32, (BLOCK, BLOCK), 0)
    col = lax.broadcasted_iota(jnp.int32, (BLOCK, BLOCK), 1)
    gap = (row - col).astype(F32)
    for h in range(heads):
        f, b = ldf[:, h * HEAD : h * HEAD + 1], ldb[:, h * HEAD : h * HEAD + 1]
        decay[h * BLOCK : (h + 1) * BLOCK] = jnp.where(
            gap >= 0, jnp.exp(f * jnp.maximum(gap, 0.0)), 0.0
        ) + jnp.where(gap <= 0, jnp.exp(b * jnp.maximum(-gap, 0.0)), 0.0)

    along_y.wait(ybuf)
    ysum[...] = sum(ybuf[k] for k in range(ny))
    along_z.start(lambda there: ysum, zbuf)
    zbuf[z] = ysum[...]
    wb = Line(at, "sp_0", nz, wb_send, wb_recv)
    wb.start(lambda there: w_zy.at[y, z], w_zy.at[y])
    spread_rows.forward()
    along_z.wait(zbuf)
    zsum[...] = sum(zbuf[k] for k in range(nz))
    sent = []
    for k, peer in enumerate(tps):
        copy = remote(zsum, tbuf.at[t], t_send.at[k], t_recv.at[t], peer)
        copy.start()
        sent.append(copy)
    tbuf[t] = zsum[...]
    wa.wait(w_yz.at[z])
    wc = Line(at, "sp_0", nz, wc_send, wc_recv)
    wc.start(lambda there: w_yz.at[z], w_yz)
    wb.wait(w_zy.at[y])
    wd = Line(at, "sp_1", ny, wd_send, wd_recv)
    wd.start(lambda there: w_zy.at[y], w_zy)
    spread_rows.finish()

    def root(rows):
        wide = rows.astype(F32)
        return lax.rsqrt(jnp.mean(wide * wide, axis=-1, keepdims=True) + EPSILON)

    @pl.loop(0, tokens // 64)
    def _(i):
        rows = pl.ds(pl.multiple_of(i * 64, 64), 64)
        stat[rows] = jnp.broadcast_to(root(rows_all[rows]), (64, 128))

    ctx_root = root(ctx_ref[...])
    for k, peer in enumerate(tps):
        s = peer.get("tp_0", x) * 2 + peer["tp_1"]
        remote(tbuf.at[s], tbuf.at[s], t_send.at[k], t_recv.at[s], peer).wait_recv()
    for s in range(nt):
        mod[:, s * 256 : (s + 1) * 256] = tbuf[s]

    def norm(rows, r, k):
        scale = gain_ref[...] * (1.0 + mod[3 * k + 1 : 3 * k + 2])
        return (rows.astype(F32) * r * scale + mod[3 * k : 3 * k + 1]).astype(BF16)

    @pl.loop(0, tokens // 64)
    def _(i):
        rows = pl.ds(pl.multiple_of(i * 64, 64), 64)
        normed[rows] = norm(rows_all[rows], stat[rows][:, 0:1], 0)

    normed[tokens : tokens + ctx_rows] = norm(ctx_ref[...], ctx_root, 1)
    weights[0].wait()
    k_all = jnp.dot(normed[...], wk[...], preferred_element_type=F32)
    weights[1].wait()
    v_all = jnp.dot(normed[...], wv[...], preferred_element_type=F32).astype(BF16)
    v_s[...] = v_all[:tokens]
    k_s[...] = rotated(k_all[:tokens], cos_s[...], sin_s[...], low).astype(BF16)
    ck = rotated(k_all[tokens:], ccos, csin, low).astype(BF16).astype(F32)
    cv = v_all[tokens:]
    spot = (sp * ctx_rows + lax.broadcasted_iota(jnp.int32, (ctx_rows, 1), 0)).astype(F32)
    cf = squeezed(outer(ck * jnp.exp(ldf * (ctx_len - 1.0 - spot)), cv), masks)
    cb = squeezed(outer(ck * jnp.exp(ldb * spot), cv), masks)
    l = lax.broadcasted_iota(jnp.int32, (BLOCK, 1), 0).astype(F32)
    to_end, to_start = jnp.exp(ldf * (BLOCK - 1.0 - l)), jnp.exp(ldb * l)
    gf, gb = jnp.exp(ldf * BLOCK), jnp.exp(ldb * BLOCK)
    sf = jnp.zeros((HEAD, width), F32)
    ub = []
    for b in range(blocks):
        keys = k_s[b * BLOCK : (b + 1) * BLOCK].astype(F32)
        values = v_s[b * BLOCK : (b + 1) * BLOCK]
        u_s[b] = sf
        sf = gf * sf + squeezed(outer(keys * to_end, values), masks)
        ub.append(squeezed(outer(keys * to_start, values), masks))
    sb = jnp.zeros((HEAD, width), F32)
    for b in reversed(range(blocks)):
        u_s[blocks + b] = sb
        sb = gb * sb + ub[b]
    for s in range(ny):
        rows = slice(s * part, (s + 1) * part)
        st[s] = jnp.concatenate([sf[rows], sb[rows], cf[rows], cb[rows]], axis=0).astype(BF16)
    one = Line(at, "sp_1", ny, a_send, a_recv)
    one.start(lambda there: st.at[there], r1)
    r1[y] = st[y]

    weights[2].wait()
    q_all = jnp.dot(normed[0:tokens], wq[...], preferred_element_type=F32)
    queries = (rotated(q_all, cos_s[...], sin_s[...], low) * HEAD ** (-0.5)).astype(BF16)
    read_f, read_b = jnp.exp(ldf * (l + 1.0)), jnp.exp(ldb * (BLOCK - l))
    for i in range(blocks):
        rows = slice(i * BLOCK, (i + 1) * BLOCK)
        wide = queries[rows].astype(F32)
        stacked = jnp.concatenate([jnp.where(m, wide, 0.0) for m in masks], axis=0).astype(BF16)
        scores = lax.dot_general(
            stacked, k_s[rows], (((1,), (1,)), ((), ())), preferred_element_type=F32
        )
        inside = jnp.dot(
            (scores * decay[...]).astype(BF16), v_s[rows], preferred_element_type=F32
        )
        states = jnp.concatenate(
            [spread_out(u_s[i], masks), spread_out(u_s[blocks + i], masks)], axis=0
        ).astype(BF16)
        near_f, near_b = wide * read_f, wide * read_b
        o = jnp.dot(
            jnp.concatenate([near_f, near_b], axis=1).astype(BF16), states,
            preferred_element_type=F32,
        )
        for h, m in enumerate(masks):
            o = o + jnp.where(m, inside[h * BLOCK : (h + 1) * BLOCK], 0.0)
        o_s[rows] = o
        far_f = wide * jnp.exp(ldf * (l + (i * BLOCK + 1.0)))
        far_b = wide * jnp.exp(ldb * ((tokens - i * BLOCK) - l))
        readers[rows] = jnp.concatenate([far_f, far_b], axis=1).astype(BF16)

    one.wait(r1)
    got = [r1[j].astype(F32) for j in range(ny)]
    hf, hb = jnp.exp(ldf * tokens), jnp.exp(ldb * tokens)
    ahead = [jnp.zeros_like(got[0][:part])]
    for j in range(ny):
        ahead.append(hf * ahead[-1] + got[j][:part])
    total_f = ahead.pop()
    behind = [jnp.zeros_like(ahead[0])]
    for j in reversed(range(ny)):
        behind.append(hb * behind[-1] + got[j][part : 2 * part])
    total_b = behind.pop()
    behind = behind[::-1]
    ctx = sum(got)
    ctx_f, ctx_b = ctx[2 * part : 3 * part], ctx[3 * part :]
    span = float(tokens * ny)
    for k in range(nz):
        there = lax.rem(z + k, nz)
        ahead_by = (there - z).astype(F32)
        to_f = jnp.where(there > z, 1.0, 0.0) * jnp.exp(ldf * (span * jnp.maximum(ahead_by - 1.0, 0.0)))
        to_b = jnp.where(there < z, 1.0, 0.0) * jnp.exp(ldb * (span * jnp.maximum(-ahead_by - 1.0, 0.0)))
        start_f = jnp.exp(ldf * (span * there.astype(F32)))
        start_b = jnp.exp(ldb * (span * (nz - 1 - there).astype(F32)))
        s2[there] = jnp.concatenate(
            [to_f * total_f + start_f * ctx_f, to_b * total_b + start_b * ctx_b], axis=0
        ).astype(BF16)
    two = Line(at, "sp_0", nz, b_send, b_recv)
    two.start(lambda there: s2.at[there], r2)
    r2[z] = s2[z]
    wc.wait(w_yz)
    two.wait(r2)
    entering = sum(r2[j].astype(F32) for j in range(nz))
    for j in range(ny):
        s3[j] = jnp.concatenate(
            [
                ahead[j] + jnp.exp(ldf * float(tokens * j)) * entering[:part],
                behind[j] + jnp.exp(ldb * float(tokens * (ny - 1 - j))) * entering[part:],
            ],
            axis=0,
        ).astype(BF16)
    three = Line(at, "sp_1", ny, c_send, c_recv)
    three.start(lambda there: s3.at[there], ent)
    ent[y] = s3[y]
    wd.wait(w_zy)
    for a in range(nz):
        for b in range(ny):
            first = (a * ny + b) * wrows
            wall[first : first + wrows, 0:128] = w_yz[a, b]
            wall[first : first + wrows, 128:256] = w_zy[b, a]
    a = lax.broadcasted_iota(jnp.int32, (width, width), 0)
    b = lax.broadcasted_iota(jnp.int32, (width, width), 1)
    average = jnp.where(a // HEAD == b // HEAD, 1.0 / HEAD, 0.0).astype(BF16)
    three.wait(ent)

    slices = [ent[s].astype(F32) for s in range(ny)]
    states = jnp.concatenate(
        [
            spread_out(jnp.concatenate([e[:part] for e in slices], axis=0), masks),
            spread_out(jnp.concatenate([e[part:] for e in slices], axis=0), masks),
        ],
        axis=0,
    ).astype(BF16)
    chunk = 2 * own
    gathers = []
    for c in range(nx):
        rows = slice(c * chunk, (c + 1) * chunk)
        o = o_s[rows] + jnp.dot(readers[rows], states, preferred_element_type=F32)
        centred = o - averaged(o, average)
        spread = averaged(centred * centred, average)
        ret[rows] = (centred * lax.rsqrt(spread + EPSILON) * hg_ref[...]).astype(BF16)
        g = Gather(
            at, nx, chunk, lambda s, a, n, c=c: gathered.at[s, pl.ds(c * chunk + a, n)],
            (g_send.at[c], g_recv.at[c]),
        )
        g.start(lambda a, n, c=c: ret.at[pl.ds(c * chunk + a, n)])
        gathers.append(g)
        gathered[t, rows] = ret[rows]
    columns = pl.ds(pl.multiple_of(t * width, width), width)
    gate_row = mod[2:3, columns]
    for g in gathers:
        g.forward()
    posted = []
    for c, g in enumerate(gathers):
        g.finish()
        rows = slice(c * chunk, (c + 1) * chunk)
        mixed = sum(
            jnp.dot(
                gathered[s, rows], wall[s * width : (s + 1) * width], preferred_element_type=F32
            )
            for s in range(nt)
        )
        result = (rows_all[rows, columns].astype(F32) + gate_row * mixed).astype(BF16)
        done[2 * c] = result[:own]
        done[2 * c + 1] = result[own:]
        for k in range(2):
            owner = 2 * c + k
            copy = remote(
                done.at[owner], landed.at[t], o_send.at[owner], o_recv.at[t],
                {"tp_0": jnp.int32(c), "tp_1": jnp.int32(k)},
            )
            other = jnp.logical_not(owner == t)

            @pl.when(other)
            def _(copy=copy):
                copy.start()

            posted.append((other, copy))
    landed[t] = done[t]
    for k, peer in enumerate(tps):
        s = peer.get("tp_0", x) * 2 + peer["tp_1"]
        remote(landed.at[s], landed.at[s], o_send.at[0], o_recv.at[s], peer).wait_recv()
    for s in range(nt):
        out_ref[:, s * width : (s + 1) * width] = landed[s]
    for line in (along_y, along_z, wa, wb, wc, wd, one, two, three, spread_rows, *gathers):
        line.drain()
    for copy in sent:
        copy.wait_send()
    for other, copy in posted:

        @pl.when(other)
        def _(copy=copy):
            copy.wait_send()


def turns(positions):
    frequency = ROTARY_BASE ** -np.linspace(0.0, 1.0, HALF)
    angles = np.asarray(positions, np.float64)[:, None] * frequency[None]
    tile = lambda a: np.tile(np.asarray(a, np.float32), (1, 128 // HALF))
    return tile(np.cos(angles)), tile(np.sin(angles))


def per_device(
    sizes, latent, context, condition, context_condition, modulation_weight, norm_gain,
    query_weight, key_weight, value_weight, log_decay, head_gain, output_weight,
):
    ny, nz, nx = sizes
    nt = 2 * nx
    d = latent.shape[1]
    width = query_weight.shape[1]
    heads = width // HEAD
    own = latent.shape[0]
    tokens = own * nt
    ctx_rows = context.shape[0]
    ctx_len = ctx_rows * ny * nz
    wrows = output_weight.shape[0]
    cos_off, sin_off = turns(np.arange(tokens))
    bases = np.stack(
        turns(ctx_len + tokens * np.arange(ny * nz)) + turns(ctx_rows * np.arange(ny * nz)), axis=1
    )
    cond = jnp.concatenate(
        [condition[None], context_condition[None], jnp.zeros((6, d), F32)], axis=0
    )
    ins = [
        cond, modulation_weight, latent, context, output_weight, norm_gain.reshape(1, d),
        log_decay, head_gain.reshape(1, width), jnp.asarray(cos_off), jnp.asarray(sin_off),
        jnp.asarray(bases), query_weight, key_weight, value_weight,
    ]
    dma = lambda *n: pltpu.SemaphoreType.DMA(n)
    part, blocks = HEAD // ny, tokens // BLOCK
    pair = lambda n: [dma(n), dma(n)]
    scratch = [
        pltpu.VMEM(shape, kind)
        for shape, kind in (
            *[((d, width), BF16)] * 3,
            ((8, width), F32), ((8, d), F32), ((tokens, d), BF16), ((tokens, 128), F32),
            ((tokens + ctx_rows, d), BF16), ((tokens, width), F32), ((tokens, width), F32),
            ((heads * BLOCK, BLOCK), F32),
            ((ny, 8, width), F32), ((nz, 8, width), F32), ((nt, 8, width), F32),
            ((8, width), F32), ((8, width), F32),
            ((nz, ny, wrows, 128), BF16), ((ny, nz, wrows, 128), BF16), ((d, width), BF16),
            ((tokens, width), BF16), ((tokens, width), BF16), ((2 * blocks, HEAD, width), F32),
            ((tokens, width), F32), ((tokens, 2 * width), BF16),
            ((ny, 4 * part, width), BF16), ((ny, 4 * part, width), BF16),
            ((nz, 2 * part, width), BF16), ((nz, 2 * part, width), BF16),
            ((ny, 2 * part, width), BF16), ((ny, 2 * part, width), BF16),
            ((tokens, width), BF16), ((nt, tokens, width), BF16),
            ((nt, own, width), BF16), ((nt, own, width), BF16),
        )
    ] + [
        dma(3), *pair(ny), *pair(nz), *pair(nt), *pair(GATHER_SEMS),
        *pair(ny), *pair(nz), *pair(nz), *pair(ny),
        *pair(ny), *pair(nz), *pair(ny), dma(nx, GATHER_SEMS), dma(nx, GATHER_SEMS), *pair(nt),
    ]
    near = pl.BlockSpec(memory_space=pltpu.VMEM)
    return pl.pallas_call(
        functools.partial(whole_kernel, sizes, ctx_len),
        out_shape=jax.ShapeDtypeStruct((own, d), BF16),
        in_specs=[near] * (len(ins) - 3) + [pl.BlockSpec(memory_space=pl.ANY)] * 3,
        out_specs=near,
        scratch_shapes=scratch,
        compiler_params=pltpu.CompilerParams(
            vmem_limit_bytes=VMEM_LIMIT, collective_id=0, has_side_effects=True
        ),
    )(*ins)


def solution(mesh, ny=8, nz=8, nx=4):
    split = Mesh(mesh.devices.reshape(nz, ny, nx, 2), SP_TP)
    placed = (
        P(SP_TP, None), P(SP, None), P(), P(), P(SP, None, TP), P(), P(None, TP), P(None, TP),
        P(None, TP), P(None, TP), P(TP), P(SP, None),
    )
    return jax.shard_map(
        functools.partial(per_device, (ny, nz, nx)), mesh=split, in_specs=placed,
        out_specs=P(SP_TP, None), check_vma=False,
    )
```

time: 111 us -> 76.8 us (0.69)
  the two profiles are of different devices: /device:TPU:7 before, /device:TPU:1 now
where the time goes in v2:
time: 76.8 us; the launch traced here: 75.9 us
  Pallas kernels  72.1 us (94%)
  local copies, waits for them, and re-layouts  2.42 us (3%)
  other arithmetic  1.42 us (2%)
    pallas_call x1, Pallas kernels, per_device(): pl.pallas_call(functools.partial(whole_kernel, sizes, ctx_len), out_shape...  72.1 us
    unnamed x4, local copies, waits for them, and re-layouts  2.34 us

profile of v2, /device:TPU:1, one launch (start us, length us, event | category | flops | bytes accessed | tf_op | source)
XLA Modules:
  0.0 75.9 jit_solution(16054891676158167080)
XLA Ops:
  0.0 0.0 copy-start
  0.0 0.1 pad.2.clone
  0.1 1.4 %maximum_maximum_fusion.cond_ref = f32[8,2048]{1,0:T(8,128)} fusion(f32[1,2048]{1,0:T(1,128)} %bitcast.5, f32[1,2048]{1,0:T(1,128)} %bitcast.6, f32[8]{0:T(128)S(1)} %pad.2.clone), kind=kLoop, calls=%fused_computation | loop fusion | flops 32768 | bytes 81952 | tf_op jit(solution)/shard_map/concatenate | solution.py:520
  1.5 0.0 copy-done
  1.5 0.7 copy.16.mw_ref
  2.2 72.1 %shard_map.145 = bf16[64,2048]{1,0:T(8,128)(2,1)} custom-call(f32[8,2048]{1,0:T(8,128)} %maximum_maximum_fusion.cond_ref, bf16[32,3,256]{2,1,0:T(4,128)(2,1)} %copy.16.mw_ref, bf16[64,2048]{1,0:T(8,128)(2,1)} %lat_ref.1, bf16[16,2048]{1,0:T(8,128)(2,1)} %ctx_ref.1, bf16[32,2048]{1,0:T(8,128)(2,1)} %w_ref.1, f32[1,2048]{1,0:T(1,128)} %bitcast.4, ...), custom_call_target="tpu_custom_call" | custom-call | tf_op jit(solution)/shard_map/pallas_call | solution.py:555
  74.3 1.7 %copy.18 = bf16[64,2048]{1,0:T(8,128)(2,1)} copy(bf16[64,2048]{1,0:T(8,128)(2,1)} %shard_map.145) | data formatting | bytes 524288
  (1 shorter events, 0.0 us)
Async XLA Ops:
  0.0 1.5 %copy-start = (bf16[32,3,256]{2,0,1:T(8,128)(2,1)S(1)}, bf16[32,3,256]{2,0,1:T(8,128)(2,1)}, u32[]{:S(2)}) copy-start(bf16[32,3,256]{2,0,1:T(8,128)(2,1)} %param.19) | copy-start | bytes 147460

commit v3 on v2

--- a/solution.py
+++ b/solution.py
@@ -178,14 +178,14 @@
 
 
 def whole_kernel(
-    sizes, ctx_len, cond_ref, mw_ref, lat_ref, ctx_ref, w_ref, gain_ref, ld_ref, hg_ref,
+    sizes, ctx_len, cond_ref, other_ref, mw_ref, lat_ref, ctx_ref, w_ref, gain_ref, ld_ref, hg_ref,
     cos_ref, sin_ref, base_ref, wq_hbm, wk_hbm, wv_hbm, out_ref,
     wq, wk, wv, part_s, mod, rows_all, stat, normed, cos_s, sin_s, decay,
     ybuf, zbuf, tbuf, ysum, zsum, w_yz, w_zy, wall,
-    k_s, v_s, u_s, o_s, readers, st, r1, s2, r2, s3, ent, ret, gathered, done, landed,
+    k_sum, v_sum, k_s, v_s, q_s, u_s, o_s, readers, st, r1, s2, r2, s3, ent, ret, gathered, done, landed,
     wt_sem, y_send, y_recv, z_send, z_recv, t_send, t_recv, l_send, l_recv,
     wa_send, wa_recv, wb_send, wb_recv, wc_send, wc_recv, wd_send, wd_recv,
-    a_send, a_recv, b_send, b_recv, c_send, c_recv, g_send, g_recv, o_send, o_recv,
+    a_send, a_recv, b_send, b_recv, c_send, c_recv, g_send, g_recv, o_send, o_recv, x_send, x_recv,
 ):
     ny, nz, nx = sizes
     nt = 2 * nx
@@ -208,15 +208,15 @@
         copy.start()
     met = greet(line_peers(at, "sp_1", ny) + line_peers(at, "sp_0", nz) + tps)
 
-    c = cond_ref[...]
+    c = jnp.concatenate([cond_ref[...], other_ref[...], jnp.zeros((6, d), F32)], axis=0)
     activated = (c / (1.0 + jnp.exp(-c))).astype(BF16)
-    depth, _, cols = mw_ref.shape
+    _, depth, cols = mw_ref.shape
     entry = lax.broadcasted_iota(jnp.int32, (d, depth), 0)
     place_of = lax.broadcasted_iota(jnp.int32, (d, depth), 1) + sp * depth
     mine = jnp.dot(
         activated, jnp.where(entry == place_of, 1.0, 0.0).astype(BF16), preferred_element_type=F32
     ).astype(BF16)
-    parts = [jnp.dot(mine, mw_ref[:, r, :], preferred_element_type=F32) for r in range(3)]
+    parts = [jnp.dot(mine, mw_ref[r], preferred_element_type=F32) for r in range(3)]
     part_s[...] = jnp.concatenate(
         [parts[r][k : k + 1] for k in range(2) for r in range(3)] + [parts[0][2:4]], axis=0
     )
@@ -235,6 +235,8 @@
     w_zy[y, z] = w_ref[:, pl.ds(pl.multiple_of(t * 256 + 128, 128), 128)]
     wa = Line(at, "sp_1", ny, wa_send, wa_recv)
     wa.start(lambda there: w_yz.at[z, y], w_yz.at[z])
+    wb = Line(at, "sp_0", nz, wb_send, wb_recv)
+    wb.start(lambda there: w_zy.at[y, z], w_zy.at[y])
 
     lane = lax.broadcasted_iota(jnp.int32, (1, width), 1)
     low = lax.rem(lane, HEAD) < HALF
@@ -262,8 +264,9 @@
     ysum[...] = sum(ybuf[k] for k in range(ny))
     along_z.start(lambda there: ysum, zbuf)
     zbuf[z] = ysum[...]
-    wb = Line(at, "sp_0", nz, wb_send, wb_recv)
-    wb.start(lambda there: w_zy.at[y, z], w_zy.at[y])
+    wb.wait(w_zy.at[y])
+    wd = Line(at, "sp_1", ny, wd_send, wd_recv)
+    wd.start(lambda there: w_zy.at[y], w_zy)
     spread_rows.forward()
     along_z.wait(zbuf)
     zsum[...] = sum(zbuf[k] for k in range(nz))
@@ -276,9 +279,6 @@
     wa.wait(w_yz.at[z])
     wc = Line(at, "sp_0", nz, wc_send, wc_recv)
     wc.start(lambda there: w_yz.at[z], w_yz)
-    wb.wait(w_zy.at[y])
-    wd = Line(at, "sp_1", ny, wd_send, wd_recv)
-    wd.start(lambda there: w_zy.at[y], w_zy)
     spread_rows.finish()
 
     def root(rows):
@@ -291,26 +291,46 @@
         stat[rows] = jnp.broadcast_to(root(rows_all[rows]), (64, 128))
 
     ctx_root = root(ctx_ref[...])
-    for k, peer in enumerate(tps):
-        s = peer.get("tp_0", x) * 2 + peer["tp_1"]
-        remote(tbuf.at[s], tbuf.at[s], t_send.at[k], t_recv.at[s], peer).wait_recv()
-    for s in range(nt):
-        mod[:, s * 256 : (s + 1) * 256] = tbuf[s]
-
-    def norm(rows, r, k):
-        scale = gain_ref[...] * (1.0 + mod[3 * k + 1 : 3 * k + 2])
-        return (rows.astype(F32) * r * scale + mod[3 * k : 3 * k + 1]).astype(BF16)
-
-    @pl.loop(0, tokens // 64)
-    def _(i):
-        rows = pl.ds(pl.multiple_of(i * 64, 64), 64)
-        normed[rows] = norm(rows_all[rows], stat[rows][:, 0:1], 0)
-
-    normed[tokens : tokens + ctx_rows] = norm(ctx_ref[...], ctx_root, 1)
-    weights[0].wait()
-    k_all = jnp.dot(normed[...], wk[...], preferred_element_type=F32)
-    weights[1].wait()
-    v_all = jnp.dot(normed[...], wv[...], preferred_element_type=F32).astype(BF16)
+
+    def came(s):
+        remote(
+            tbuf.at[s], tbuf.at[s], t_send.at[0], t_recv.at[s], {"tp_1": 1 - core}
+        ).wait_recv()
+
+    def norm(rows, r, k, columns):
+        scale = gain_ref[:, columns] * (1.0 + mod[3 * k + 1 : 3 * k + 2, columns])
+        return (rows.astype(F32) * r * scale + mod[3 * k : 3 * k + 1, columns]).astype(BF16)
+
+    for steps in (0, 1, 3, 2):
+        chip = lax.rem(x + steps, nx)
+        came(2 * chip + 1 - core)
+        if steps:
+            came(2 * chip + core)
+        for k in range(2):
+            columns = pl.ds(pl.multiple_of(chip * 512 + k * 256, 256), 256)
+            mod[:, columns] = tbuf[2 * chip + k]
+        if steps == 0:
+            weights[0].wait()
+            weights[1].wait()
+        for k in range(2):
+            columns = pl.ds(pl.multiple_of(chip * 512 + k * 256, 256), 256)
+            r = jnp.concatenate([stat[...]] * 2, axis=1)
+            normed[0:tokens, columns] = norm(rows_all[:, columns], r, 0, columns)
+            normed[tokens : tokens + ctx_rows, columns] = norm(
+                ctx_ref[:, columns], ctx_root, 1, columns
+            )
+        columns = pl.ds(pl.multiple_of(chip * 512, 512), 512)
+        k_more = jnp.dot(normed[:, columns], wk[columns], preferred_element_type=F32)
+        v_more = jnp.dot(normed[:, columns], wv[columns], preferred_element_type=F32)
+        if steps == 0:
+            k_sum[...] = k_more
+            v_sum[...] = v_more
+        elif steps != 2:
+            k_sum[...] += k_more
+            v_sum[...] += v_more
+        else:
+            k_all = k_sum[...] + k_more
+            v_all = (v_sum[...] + v_more).astype(BF16)
     v_s[...] = v_all[:tokens]
     k_s[...] = rotated(k_all[:tokens], cos_s[...], sin_s[...], low).astype(BF16)
     ck = rotated(k_all[tokens:], ccos, csin, low).astype(BF16).astype(F32)
@@ -344,9 +364,11 @@
     q_all = jnp.dot(normed[0:tokens], wq[...], preferred_element_type=F32)
     queries = (rotated(q_all, cos_s[...], sin_s[...], low) * HEAD ** (-0.5)).astype(BF16)
     read_f, read_b = jnp.exp(ldf * (l + 1.0)), jnp.exp(ldb * (BLOCK - l))
-    for i in range(blocks):
+    q_s[...] = queries
+
+    def near(i):
         rows = slice(i * BLOCK, (i + 1) * BLOCK)
-        wide = queries[rows].astype(F32)
+        wide = q_s[rows].astype(F32)
         stacked = jnp.concatenate([jnp.where(m, wide, 0.0) for m in masks], axis=0).astype(BF16)
         scores = lax.dot_general(
             stacked, k_s[rows], (((1,), (1,)), ((), ())), preferred_element_type=F32
@@ -369,6 +391,8 @@
         far_b = wide * jnp.exp(ldb * ((tokens - i * BLOCK) - l))
         readers[rows] = jnp.concatenate([far_f, far_b], axis=1).astype(BF16)
 
+    for i in range(blocks // 2):
+        near(i)
     one.wait(r1)
     got = [r1[j].astype(F32) for j in range(ny)]
     hf, hb = jnp.exp(ldf * tokens), jnp.exp(ldb * tokens)
@@ -397,6 +421,8 @@
     two = Line(at, "sp_0", nz, b_send, b_recv)
     two.start(lambda there: s2.at[there], r2)
     r2[z] = s2[z]
+    for i in range(blocks // 2, blocks):
+        near(i)
     wc.wait(w_yz)
     two.wait(r2)
     entering = sum(r2[j].astype(F32) for j in range(nz))
@@ -415,8 +441,11 @@
     for a in range(nz):
         for b in range(ny):
             first = (a * ny + b) * wrows
-            wall[first : first + wrows, 0:128] = w_yz[a, b]
-            wall[first : first + wrows, 128:256] = w_zy[b, a]
+            wall[core, first : first + wrows, 0:128] = w_yz[a, b]
+            wall[core, first : first + wrows, 128:256] = w_zy[b, a]
+    over = {"tp_1": 1 - core}
+    w_over = remote(wall.at[core], wall.at[core], x_send.at[0], x_recv.at[0], over)
+    w_over.start()
     a = lax.broadcasted_iota(jnp.int32, (width, width), 0)
     b = lax.broadcasted_iota(jnp.int32, (width, width), 1)
     average = jnp.where(a // HEAD == b // HEAD, 1.0 / HEAD, 0.0).astype(BF16)
@@ -430,66 +459,91 @@
         ],
         axis=0,
     ).astype(BF16)
-    chunk = 2 * own
-    gathers = []
-    for c in range(nx):
-        rows = slice(c * chunk, (c + 1) * chunk)
+    order = (2, 1, 3, 0)
+    right, left = lax.rem(x + 1, nx), lax.rem(x + nx - 1, nx)
+    to_right, to_left = {"tp_0": right}, {"tp_0": left}
+    partner = t + 1 - 2 * core
+    posted = []
+
+    def post(src, dst, q, s, r, device):
+        copy = remote(src, dst, g_send.at[q, s], g_recv.at[q, r], device)
+        copy.start()
+        posted.append(copy)
+
+    def arrived(q, s, r):
+        remote(
+            gathered.at[q, s], gathered.at[q, s], g_send.at[q, 0], g_recv.at[q, r], over
+        ).wait_recv()
+
+    for steps in order:
+        q = lax.rem(x + steps, nx)
+        rows = pl.ds(pl.multiple_of(q * 2 * own, 2 * own), 2 * own)
         o = o_s[rows] + jnp.dot(readers[rows], states, preferred_element_type=F32)
         centred = o - averaged(o, average)
         spread = averaged(centred * centred, average)
-        ret[rows] = (centred * lax.rsqrt(spread + EPSILON) * hg_ref[...]).astype(BF16)
-        g = Gather(
-            at, nx, chunk, lambda s, a, n, c=c: gathered.at[s, pl.ds(c * chunk + a, n)],
-            (g_send.at[c], g_recv.at[c]),
+        kept = (centred * lax.rsqrt(spread + EPSILON) * hg_ref[...]).astype(BF16)
+        ret[2 * q] = kept[:own]
+        ret[2 * q + 1] = kept[own:]
+        post(ret.at[2 * q + 1 - core], gathered.at[q, t], q, 0, 0, over)
+        post(ret.at[2 * q + core], gathered.at[q, t], q, 1, 1 + core, to_right)
+        post(ret.at[2 * q + core], gathered.at[q, t], q, 2, 3 + core, to_left)
+        gathered[q, t] = ret[2 * q + core]
+    for steps in order:
+        q = lax.rem(x + steps, nx)
+        arrived(q, partner, 0)
+        post(gathered.at[q, partner], gathered.at[q, partner], q, 3, 2 - core, to_right)
+        post(gathered.at[q, partner], gathered.at[q, partner], q, 4, 4 - core, to_left)
+        q = lax.rem(left + steps, nx)
+        arrived(q, 2 * left, 1)
+        post(gathered.at[q, 2 * left], gathered.at[q, 2 * left], q, 5, 5, to_right)
+        q = lax.rem(right + steps, nx)
+        arrived(q, 2 * right + 1, 4)
+        post(gathered.at[q, 2 * right + 1], gathered.at[q, 2 * right + 1], q, 6, 6, to_left)
+    w_over.wait_recv()
+    far = lax.rem(x + 2, nx)
+
+    def mixed_for(qs):
+        for q in qs:
+            arrived(q, 2 * left + 1, 2)
+            arrived(q, 2 * right, 3)
+            arrived(q, 2 * far, 5)
+            arrived(q, 2 * far + 1, 6)
+        rows = jnp.concatenate(
+            [jnp.concatenate([gathered[q, s] for s in range(nt)], axis=1) for q in qs], axis=0
         )
-        g.start(lambda a, n, c=c: ret.at[pl.ds(c * chunk + a, n)])
-        gathers.append(g)
-        gathered[t, rows] = ret[rows]
-    columns = pl.ds(pl.multiple_of(t * width, width), width)
-    gate_row = mod[2:3, columns]
-    for g in gathers:
-        g.forward()
-    posted = []
-    for c, g in enumerate(gathers):
-        g.finish()
-        rows = slice(c * chunk, (c + 1) * chunk)
-        mixed = sum(
-            jnp.dot(
-                gathered[s, rows], wall[s * width : (s + 1) * width], preferred_element_type=F32
-            )
-            for s in range(nt)
-        )
-        result = (rows_all[rows, columns].astype(F32) + gate_row * mixed).astype(BF16)
-        done[2 * c] = result[:own]
-        done[2 * c + 1] = result[own:]
         for k in range(2):
-            owner = 2 * c + k
-            copy = remote(
-                done.at[owner], landed.at[t], o_send.at[owner], o_recv.at[t],
-                {"tp_0": jnp.int32(c), "tp_1": jnp.int32(k)},
-            )
-            other = jnp.logical_not(owner == t)
-
-            @pl.when(other)
-            def _(copy=copy):
-                copy.start()
-
-            posted.append((other, copy))
-    landed[t] = done[t]
-    for k, peer in enumerate(tps):
-        s = peer.get("tp_0", x) * 2 + peer["tp_1"]
-        remote(landed.at[s], landed.at[s], o_send.at[0], o_recv.at[s], peer).wait_recv()
-    for s in range(nt):
-        out_ref[:, s * width : (s + 1) * width] = landed[s]
-    for line in (along_y, along_z, wa, wb, wc, wd, one, two, three, spread_rows, *gathers):
+            columns = pl.ds(pl.multiple_of((2 * x + k) * width, width), width)
+            mixed = jnp.dot(rows, wall[k], preferred_element_type=F32)
+            for i, q in enumerate(qs):
+                mine = pl.ds(pl.multiple_of((2 * q + core) * own, own), own)
+                result = rows_all[mine, columns].astype(F32) + mod[2:3, columns] * mixed[
+                    i * own : (i + 1) * own
+                ]
+                done[q, :, k * width : (k + 1) * width] = result.astype(BF16)
+
+    def give(steps):
+        q = lax.rem(x + steps, nx)
+        copy = remote(done.at[q], landed.at[x], o_send.at[steps], o_recv.at[x], {"tp_0": q})
+        copy.start()
+        posted.append(copy)
+
+    mixed_for([far])
+    give(2)
+    mixed_for([right, left])
+    give(1)
+    give(nx - 1)
+    mixed_for([x])
+    landed[x] = done[x]
+    for chip in (right, left, far):
+        remote(
+            landed.at[chip], landed.at[chip], o_send.at[0], o_recv.at[chip], {"tp_0": chip}
+        ).wait_recv()
+    for chip in range(nx):
+        out_ref[:, chip * 2 * width : (chip + 1) * 2 * width] = landed[chip]
+    for line in (along_y, along_z, wa, wb, wc, wd, one, two, three, spread_rows):
         line.drain()
-    for copy in sent:
+    for copy in sent + posted + [w_over]:
         copy.wait_send()
-    for other, copy in posted:
-
-        @pl.when(other)
-        def _(copy=copy):
-            copy.wait_send()
 
 
 def turns(positions):
@@ -517,11 +571,9 @@
     bases = np.stack(
         turns(ctx_len + tokens * np.arange(ny * nz)) + turns(ctx_rows * np.arange(ny * nz)), axis=1
     )
-    cond = jnp.concatenate(
-        [condition[None], context_condition[None], jnp.zeros((6, d), F32)], axis=0
-    )
     ins = [
-        cond, modulation_weight, latent, context, output_weight, norm_gain.reshape(1, d),
+        condition.reshape(1, d), context_condition.reshape(1, d),
+        modulation_weight.transpose(1, 0, 2), latent, context, output_weight, norm_gain.reshape(1, d),
         log_decay, head_gain.reshape(1, width), jnp.asarray(cos_off), jnp.asarray(sin_off),
         jnp.asarray(bases), query_weight, key_weight, value_weight,
     ]
@@ -537,19 +589,21 @@
             ((heads * BLOCK, BLOCK), F32),
             ((ny, 8, width), F32), ((nz, 8, width), F32), ((nt, 8, width), F32),
             ((8, width), F32), ((8, width), F32),
-            ((nz, ny, wrows, 128), BF16), ((ny, nz, wrows, 128), BF16), ((d, width), BF16),
-            ((tokens, width), BF16), ((tokens, width), BF16), ((2 * blocks, HEAD, width), F32),
+            ((nz, ny, wrows, 128), BF16), ((ny, nz, wrows, 128), BF16), ((2, d, width), BF16),
+            ((tokens + ctx_rows, width), F32), ((tokens + ctx_rows, width), F32),
+            ((tokens, width), BF16), ((tokens, width), BF16), ((tokens, width), BF16),
+            ((2 * blocks, HEAD, width), F32),
             ((tokens, width), F32), ((tokens, 2 * width), BF16),
             ((ny, 4 * part, width), BF16), ((ny, 4 * part, width), BF16),
             ((nz, 2 * part, width), BF16), ((nz, 2 * part, width), BF16),
             ((ny, 2 * part, width), BF16), ((ny, 2 * part, width), BF16),
-            ((tokens, width), BF16), ((nt, tokens, width), BF16),
-            ((nt, own, width), BF16), ((nt, own, width), BF16),
+            ((nt, own, width), BF16), ((nx, nt, own, width), BF16),
+            ((nx, own, 2 * width), BF16), ((nx, own, 2 * width), BF16),
         )
     ] + [
         dma(3), *pair(ny), *pair(nz), *pair(nt), *pair(GATHER_SEMS),
         *pair(ny), *pair(nz), *pair(nz), *pair(ny),
-        *pair(ny), *pair(nz), *pair(ny), dma(nx, GATHER_SEMS), dma(nx, GATHER_SEMS), *pair(nt),
+        *pair(ny), *pair(nz), *pair(ny), dma(nx, 7), dma(nx, 7), *pair(nx), *pair(1),
     ]
     near = pl.BlockSpec(memory_space=pltpu.VMEM)
     return pl.pallas_call(

time: 76.8 us -> 76.9 us (level)
  the two profiles are of different devices: /device:TPU:1 before, /device:TPU:8 now
where the time goes in v3:
time: 76.9 us; the launch traced here: 76.7 us
  Pallas kernels  75 us (98%)
  local copies, waits for them, and re-layouts  1.67 us (2%)
    pallas_call x1, Pallas kernels, per_device(): pl.pallas_call(functools.partial(whole_kernel, sizes, ctx_len), out_shape...  75 us
    unnamed x1, local copies, waits for them, and re-layouts  1.67 us

profile of v3, /device:TPU:8, one launch (start us, length us, event | category | flops | bytes accessed | tf_op | source)
XLA Modules:
  0.0 76.7 jit_solution(6918006242744331885)
XLA Ops:
  0.0 75.0 %shard_map.145 = bf16[64,2048]{1,0:T(8,128)(2,1)} custom-call(f32[1,2048]{1,0:T(1,128)} %bitcast.6, f32[1,2048]{1,0:T(1,128)} %bitcast.7, bf16[3,32,256]{2,1,0:T(8,128)(2,1)} %bitcast.5, bf16[64,2048]{1,0:T(8,128)(2,1)} %lat_ref.1, bf16[16,2048]{1,0:T(8,128)(2,1)} %ctx_ref.1, bf16[32,2048]{1,0:T(8,128)(2,1)} %w_ref.1, f32[1,2048]{1,0:T(1,128)} %bitcast.8, ...), custom_call_target="tpu_custom_call" | custom-call | tf_op jit(solution)/shard_map/pallas_call | solution.py:609
  75.0 1.7 %copy.17 = bf16[64,2048]{1,0:T(8,128)(2,1)} copy(bf16[64,2048]{1,0:T(8,128)(2,1)} %shard_map.145) | data formatting | bytes 524288

commit v4 on v3

--- a/solution.py
+++ b/solution.py
@@ -364,6 +364,9 @@
     q_all = jnp.dot(normed[0:tokens], wq[...], preferred_element_type=F32)
     queries = (rotated(q_all, cos_s[...], sin_s[...], low) * HEAD ** (-0.5)).astype(BF16)
     read_f, read_b = jnp.exp(ldf * (l + 1.0)), jnp.exp(ldb * (BLOCK - l))
+    a = lax.broadcasted_iota(jnp.int32, (width, width), 0)
+    b = lax.broadcasted_iota(jnp.int32, (width, width), 1)
+    average = jnp.where(a // HEAD == b // HEAD, 1.0 / HEAD, 0.0).astype(BF16)
     q_s[...] = queries
 
     def near(i):
@@ -386,7 +389,7 @@
         )
         for h, m in enumerate(masks):
             o = o + jnp.where(m, inside[h * BLOCK : (h + 1) * BLOCK], 0.0)
-        o_s[rows] = o
+        o_s[rows] = o - averaged(o, average)
         far_f = wide * jnp.exp(ldf * (l + (i * BLOCK + 1.0)))
         far_b = wide * jnp.exp(ldb * ((tokens - i * BLOCK) - l))
         readers[rows] = jnp.concatenate([far_f, far_b], axis=1).astype(BF16)
@@ -446,18 +449,13 @@
     over = {"tp_1": 1 - core}
     w_over = remote(wall.at[core], wall.at[core], x_send.at[0], x_recv.at[0], over)
     w_over.start()
-    a = lax.broadcasted_iota(jnp.int32, (width, width), 0)
-    b = lax.broadcasted_iota(jnp.int32, (width, width), 1)
-    average = jnp.where(a // HEAD == b // HEAD, 1.0 / HEAD, 0.0).astype(BF16)
     three.wait(ent)
 
     slices = [ent[s].astype(F32) for s in range(ny)]
+    packed = jnp.concatenate([e[:part] for e in slices] + [e[part:] for e in slices], axis=0)
+    packed = packed - averaged(packed, average)
     states = jnp.concatenate(
-        [
-            spread_out(jnp.concatenate([e[:part] for e in slices], axis=0), masks),
-            spread_out(jnp.concatenate([e[part:] for e in slices], axis=0), masks),
-        ],
-        axis=0,
+        [spread_out(packed[:HEAD], masks), spread_out(packed[HEAD:], masks)], axis=0
     ).astype(BF16)
     order = (2, 1, 3, 0)
     right, left = lax.rem(x + 1, nx), lax.rem(x + nx - 1, nx)
@@ -478,8 +476,7 @@
     for steps in order:
         q = lax.rem(x + steps, nx)
         rows = pl.ds(pl.multiple_of(q * 2 * own, 2 * own), 2 * own)
-        o = o_s[rows] + jnp.dot(readers[rows], states, preferred_element_type=F32)
-        centred = o - averaged(o, average)
+        centred = o_s[rows] + jnp.dot(readers[rows], states, preferred_element_type=F32)
         spread = averaged(centred * centred, average)
         kept = (centred * lax.rsqrt(spread + EPSILON) * hg_ref[...]).astype(BF16)
         ret[2 * q] = kept[:own]
@@ -493,6 +490,7 @@
         arrived(q, partner, 0)
         post(gathered.at[q, partner], gathered.at[q, partner], q, 3, 2 - core, to_right)
         post(gathered.at[q, partner], gathered.at[q, partner], q, 4, 4 - core, to_left)
+    for steps in order:
         q = lax.rem(left + steps, nx)
         arrived(q, 2 * left, 1)
         post(gathered.at[q, 2 * left], gathered.at[q, 2 * left], q, 5, 5, to_right)

time: 76.9 us -> 68 us (0.88)
  the two profiles are of different devices: /device:TPU:8 before, /device:TPU:1 now
where the time goes in v4:
time: 68 us; the launch traced here: 67.8 us
  Pallas kernels  66.1 us (97%)
  local copies, waits for them, and re-layouts  1.67 us (2%)
    pallas_call x1, Pallas kernels, per_device(): pl.pallas_call(functools.partial(whole_kernel, sizes, ctx_len), out_shape...  66.1 us
    unnamed x1, local copies, waits for them, and re-layouts  1.67 us

profile of v4, /device:TPU:1, one launch (start us, length us, event | category | flops | bytes accessed | tf_op | source)
XLA Modules:
  0.0 67.8 jit_solution(4010917724844168791)
XLA Ops:
  0.0 66.1 %shard_map.145 = bf16[64,2048]{1,0:T(8,128)(2,1)} custom-call(f32[1,2048]{1,0:T(1,128)} %bitcast.6, f32[1,2048]{1,0:T(1,128)} %bitcast.7, bf16[3,32,256]{2,1,0:T(8,128)(2,1)} %bitcast.5, bf16[64,2048]{1,0:T(8,128)(2,1)} %lat_ref.1, bf16[16,2048]{1,0:T(8,128)(2,1)} %ctx_ref.1, bf16[32,2048]{1,0:T(8,128)(2,1)} %w_ref.1, f32[1,2048]{1,0:T(1,128)} %bitcast.8, ...), custom_call_target="tpu_custom_call" | custom-call | tf_op jit(solution)/shard_map/pallas_call | solution.py:607
  66.1 1.7 %copy.17 = bf16[64,2048]{1,0:T(8,128)(2,1)} copy(bf16[64,2048]{1,0:T(8,128)(2,1)} %shard_map.145) | data formatting | bytes 524288

commit v5 on v4

--- a/solution.py
+++ b/solution.py
@@ -35,10 +35,12 @@
 
 def tp_peers(at, nx):
     core, x = at["tp_1"], at["tp_0"]
-    peers = [{"tp_0": x, "tp_1": 1 - core}]
-    for k in range(1, nx):
-        there = lax.rem(x + k, nx)
-        peers += [{"tp_0": there, "tp_1": core}, {"tp_0": there, "tp_1": 1 - core}]
+    peers = []
+    for k in sorted(range(1, nx), key=lambda k: -min(k, nx - k)):
+        peers.append({"tp_0": lax.rem(x + k, nx), "tp_1": 1 - core})
+    peers.append({"tp_0": x, "tp_1": 1 - core})
+    for k in sorted(range(1, nx), key=lambda k: -min(k, nx - k)):
+        peers.append({"tp_0": lax.rem(x + k, nx), "tp_1": core})
     return peers
 
 
@@ -60,7 +62,7 @@
         self.sent = []
 
     def start(self, source_of, slots):
-        for k in range(1, self.n):
+        for k in sorted(range(1, self.n), key=lambda k: -min(k, self.n - k)):
             there = lax.rem(self.me + k, self.n)
             copy = remote(
                 source_of(there), slots.at[self.me], self.send_sems.at[k],
@@ -179,8 +181,8 @@
 
 def whole_kernel(
     sizes, ctx_len, cond_ref, other_ref, mw_ref, lat_ref, ctx_ref, w_ref, gain_ref, ld_ref, hg_ref,
-    cos_ref, sin_ref, base_ref, wq_hbm, wk_hbm, wv_hbm, out_ref,
-    wq, wk, wv, part_s, mod, rows_all, stat, normed, cos_s, sin_s, decay,
+    cos_hbm, sin_hbm, base_hbm, wq_hbm, wk_hbm, wv_hbm, out_ref,
+    cos_ref, sin_ref, base_ref, wq, wk, wv, part_s, mod, rows_all, stat, normed, cos_s, sin_s, decay,
     ybuf, zbuf, tbuf, ysum, zsum, w_yz, w_zy, wall,
     k_sum, v_sum, k_s, v_s, q_s, u_s, o_s, readers, st, r1, s2, r2, s3, ent, ret, gathered, done, landed,
     wt_sem, y_send, y_recv, z_send, z_recv, t_send, t_recv, l_send, l_recv,
@@ -200,13 +202,16 @@
     y, z, x, core = at["sp_1"], at["sp_0"], at["tp_0"], at["tp_1"]
     t, sp = x * 2 + core, z * ny + y
     tps = tp_peers(at, nx)
+    met = greet(line_peers(at, "sp_1", ny) + line_peers(at, "sp_0", nz) + tps)
+    fetched = (
+        (wk_hbm, wk), (wv_hbm, wv), (wq_hbm, wq),
+        (cos_hbm, cos_ref), (sin_hbm, sin_ref), (base_hbm.at[sp], base_ref),
+    )
     weights = [
-        pltpu.make_async_copy(a, b, wt_sem.at[i])
-        for i, (a, b) in enumerate(((wk_hbm, wk), (wv_hbm, wv), (wq_hbm, wq)))
+        pltpu.make_async_copy(a, b, wt_sem.at[i]) for i, (a, b) in enumerate(fetched)
     ]
-    for copy in weights:
+    for copy in weights[3:] + weights[:3]:
         copy.start()
-    met = greet(line_peers(at, "sp_1", ny) + line_peers(at, "sp_0", nz) + tps)
 
     c = jnp.concatenate([cond_ref[...], other_ref[...], jnp.zeros((6, d), F32)], axis=0)
     activated = (c / (1.0 + jnp.exp(-c))).astype(BF16)
@@ -242,7 +247,9 @@
     low = lax.rem(lane, HEAD) < HALF
     sign = jnp.where(low, -1.0, 1.0)
     repeat = lambda a: jnp.concatenate([a] * (width // a.shape[1]), axis=1)
-    base = repeat(base_ref[sp])
+    for copy in weights[3:]:
+        copy.wait()
+    base = repeat(base_ref[...])
     cos_off, sin_off = repeat(cos_ref[...]), repeat(sin_ref[...])
     cos_s[...] = base[0:1] * cos_off - base[1:2] * sin_off
     sin_s[...] = (base[1:2] * cos_off + base[0:1] * sin_off) * sign
@@ -396,6 +403,16 @@
 
     for i in range(blocks // 2):
         near(i)
+    span = float(tokens * ny)
+    factors = []
+    for k in range(nz):
+        there = lax.rem(z + k, nz)
+        ahead_by = (there - z).astype(F32)
+        to_f = jnp.where(there > z, 1.0, 0.0) * jnp.exp(ldf * (span * jnp.maximum(ahead_by - 1.0, 0.0)))
+        to_b = jnp.where(there < z, 1.0, 0.0) * jnp.exp(ldb * (span * jnp.maximum(-ahead_by - 1.0, 0.0)))
+        start_f = jnp.exp(ldf * (span * there.astype(F32)))
+        start_b = jnp.exp(ldb * (span * (nz - 1 - there).astype(F32)))
+        factors.append((there, to_f, to_b, start_f, start_b))
     one.wait(r1)
     got = [r1[j].astype(F32) for j in range(ny)]
     hf, hb = jnp.exp(ldf * tokens), jnp.exp(ldb * tokens)
@@ -410,14 +427,7 @@
     behind = behind[::-1]
     ctx = sum(got)
     ctx_f, ctx_b = ctx[2 * part : 3 * part], ctx[3 * part :]
-    span = float(tokens * ny)
-    for k in range(nz):
-        there = lax.rem(z + k, nz)
-        ahead_by = (there - z).astype(F32)
-        to_f = jnp.where(there > z, 1.0, 0.0) * jnp.exp(ldf * (span * jnp.maximum(ahead_by - 1.0, 0.0)))
-        to_b = jnp.where(there < z, 1.0, 0.0) * jnp.exp(ldb * (span * jnp.maximum(-ahead_by - 1.0, 0.0)))
-        start_f = jnp.exp(ldf * (span * there.astype(F32)))
-        start_b = jnp.exp(ldb * (span * (nz - 1 - there).astype(F32)))
+    for there, to_f, to_b, start_f, start_b in factors:
         s2[there] = jnp.concatenate(
             [to_f * total_f + start_f * ctx_f, to_b * total_b + start_b * ctx_b], axis=0
         ).astype(BF16)
@@ -581,6 +591,7 @@
     scratch = [
         pltpu.VMEM(shape, kind)
         for shape, kind in (
+            ((tokens, 128), F32), ((tokens, 128), F32), ((4, 128), F32),
             *[((d, width), BF16)] * 3,
             ((8, width), F32), ((8, d), F32), ((tokens, d), BF16), ((tokens, 128), F32),
             ((tokens + ctx_rows, d), BF16), ((tokens, width), F32), ((tokens, width), F32),
@@ -599,15 +610,15 @@
             ((nx, own, 2 * width), BF16), ((nx, own, 2 * width), BF16),
         )
     ] + [
-        dma(3), *pair(ny), *pair(nz), *pair(nt), *pair(GATHER_SEMS),
+        dma(6), *pair(ny), *pair(nz), *pair(nt), *pair(GATHER_SEMS),
         *pair(ny), *pair(nz), *pair(nz), *pair(ny),
         *pair(ny), *pair(nz), *pair(ny), dma(nx, 7), dma(nx, 7), *pair(nx), *pair(1),
     ]
     near = pl.BlockSpec(memory_space=pltpu.VMEM)
     return pl.pallas_call(
         functools.partial(whole_kernel, sizes, ctx_len),
-        out_shape=jax.ShapeDtypeStruct((own, d), BF16),
-        in_specs=[near] * (len(ins) - 3) + [pl.BlockSpec(memory_space=pl.ANY)] * 3,
+        out_shape=pltpu.VMEM((own, d), BF16),
+        in_specs=[near] * (len(ins) - 6) + [pl.BlockSpec(memory_space=pl.ANY)] * 6,
         out_specs=near,
         scratch_shapes=scratch,
         compiler_params=pltpu.CompilerParams(

time: 68 us -> 65.5 us (0.963); the launches traced: 67.8 us -> 64.6 us
  Pallas kernels: 66.1 us -> 63.8 us
  local copies, waits for them, and re-layouts: 1.67 us -> 0.71 us
    pallas_call x1, Pallas kernels: 66.1 us -> 63.8 us  [per_device(): pl.pallas_call(functools.partial(whole_kernel, sizes, ctx_len), out_shape...]
    unnamed x1, local copies, waits for them, and re-layouts: 1.67 us -> 0.71 us
where the time goes in v5:
time: 65.5 us; the launch traced here: 64.6 us
  Pallas kernels  63.8 us (97%)
  local copies, waits for them, and re-layouts  0.71 us (1%)
    pallas_call x1, Pallas kernels, per_device(): pl.pallas_call(functools.partial(whole_kernel, sizes, ctx_len), out_shape...  63.8 us

profile of v5, /device:TPU:1, one launch (start us, length us, event | category | flops | bytes accessed | tf_op | source)
XLA Modules:
  0.0 64.6 jit_solution(4785931076111855449)
XLA Ops:
  0.0 63.8 %shard_map.145 = bf16[64,2048]{1,0:T(8,128)(2,1)S(1)} custom-call(f32[1,2048]{1,0:T(1,128)} %bitcast.6, f32[1,2048]{1,0:T(1,128)} %bitcast.7, bf16[3,32,256]{2,1,0:T(8,128)(2,1)} %bitcast.5, bf16[64,2048]{1,0:T(8,128)(2,1)} %lat_ref.1, bf16[16,2048]{1,0:T(8,128)(2,1)} %ctx_ref.1, bf16[32,2048]{1,0:T(8,128)(2,1)} %w_ref.1, f32[1,2048]{1,0:T(1,128)} %bitcast.8, ...), custom_call_target="tpu_custom_call" | custom-call | tf_op jit(solution)/shard_map/pallas_call | solution.py:618
  63.8 0.7 %copy.17 = bf16[64,2048]{1,0:T(8,128)(2,1)} copy(bf16[64,2048]{1,0:T(8,128)(2,1)S(1)} %shard_map.145) | data formatting | bytes 524288

commit v6 on v5

--- a/solution.py
+++ b/solution.py
@@ -184,7 +184,7 @@
     cos_hbm, sin_hbm, base_hbm, wq_hbm, wk_hbm, wv_hbm, out_ref,
     cos_ref, sin_ref, base_ref, wq, wk, wv, part_s, mod, rows_all, stat, normed, cos_s, sin_s, decay,
     ybuf, zbuf, tbuf, ysum, zsum, w_yz, w_zy, wall,
-    k_sum, v_sum, k_s, v_s, q_s, u_s, o_s, readers, st, r1, s2, r2, s3, ent, ret, gathered, done, landed,
+    k_sum, v_sum, k_s, v_s, q_s, u_s, o_s, readers, st, r1, s2, r2, s3, ent, ret, gathered, near_sum, done, landed,
     wt_sem, y_send, y_recv, z_send, z_recv, t_send, t_recv, l_send, l_recv,
     wa_send, wa_recv, wb_send, wb_recv, wc_send, wc_recv, wd_send, wd_recv,
     a_send, a_recv, b_send, b_recv, c_send, c_recv, g_send, g_recv, o_send, o_recv, x_send, x_recv,
@@ -487,7 +487,7 @@
         q = lax.rem(x + steps, nx)
         rows = pl.ds(pl.multiple_of(q * 2 * own, 2 * own), 2 * own)
         centred = o_s[rows] + jnp.dot(readers[rows], states, preferred_element_type=F32)
-        spread = averaged(centred * centred, average)
+        spread = jnp.dot((centred * centred).astype(BF16), average, preferred_element_type=F32)
         kept = (centred * lax.rsqrt(spread + EPSILON) * hg_ref[...]).astype(BF16)
         ret[2 * q] = kept[:own]
         ret[2 * q + 1] = kept[own:]
@@ -510,44 +510,61 @@
     w_over.wait_recv()
     far = lax.rem(x + 2, nx)
 
-    def mixed_for(qs):
-        for q in qs:
-            arrived(q, 2 * left + 1, 2)
-            arrived(q, 2 * right, 3)
-            arrived(q, 2 * far, 5)
-            arrived(q, 2 * far + 1, 6)
-        rows = jnp.concatenate(
-            [jnp.concatenate([gathered[q, s] for s in range(nt)], axis=1) for q in qs], axis=0
+    qs = [lax.rem(x + steps, nx) for steps in order]
+
+    def block(q, chip):
+        return jnp.concatenate([gathered[q, 2 * chip], gathered[q, 2 * chip + 1]], axis=1)
+
+    def matrix(k, chip):
+        return wall[k, pl.ds(pl.multiple_of(chip * 2 * width, 2 * width), 2 * width)]
+
+    for q in qs:
+        arrived(q, 2 * left + 1, 2)
+        arrived(q, 2 * right, 3)
+    for k in range(2):
+        near_sum[:, k * width : (k + 1) * width] = sum(
+            jnp.dot(
+                jnp.concatenate([block(q, chip) for q in qs], axis=0), matrix(k, chip),
+                preferred_element_type=F32,
+            )
+            for chip in (x, left, right)
         )
+
+    def finish(spots):
+        for i in spots:
+            arrived(qs[i], 2 * far, 5)
+            arrived(qs[i], 2 * far + 1, 6)
+        rows = jnp.concatenate([block(qs[i], far) for i in spots], axis=0)
         for k in range(2):
             columns = pl.ds(pl.multiple_of((2 * x + k) * width, width), width)
-            mixed = jnp.dot(rows, wall[k], preferred_element_type=F32)
-            for i, q in enumerate(qs):
+            more = jnp.dot(rows, matrix(k, far), preferred_element_type=F32)
+            for j, i in enumerate(spots):
+                q = qs[i]
                 mine = pl.ds(pl.multiple_of((2 * q + core) * own, own), own)
-                result = rows_all[mine, columns].astype(F32) + mod[2:3, columns] * mixed[
-                    i * own : (i + 1) * own
-                ]
-                done[q, :, k * width : (k + 1) * width] = result.astype(BF16)
-
-    def give(steps):
-        q = lax.rem(x + steps, nx)
-        copy = remote(done.at[q], landed.at[x], o_send.at[steps], o_recv.at[x], {"tp_0": q})
-        copy.start()
-        posted.append(copy)
-
-    mixed_for([far])
-    give(2)
-    mixed_for([right, left])
-    give(1)
-    give(nx - 1)
-    mixed_for([x])
+                mixed = near_sum[i * own : (i + 1) * own, k * width : (k + 1) * width]
+                mixed = mixed + more[j * own : (j + 1) * own]
+                result = rows_all[mine, columns].astype(F32) + mod[2:3, columns] * mixed
+                done[q, k] = result.astype(BF16)
+                if order[i]:
+                    copy = remote(
+                        done.at[q, k], landed.at[x, k], o_send.at[i, k], o_recv.at[x, k],
+                        {"tp_0": q},
+                    )
+                    copy.start()
+                    posted.append(copy)
+
+    finish([0])
+    finish([1, 2])
+    finish([3])
     landed[x] = done[x]
     for chip in (right, left, far):
-        remote(
-            landed.at[chip], landed.at[chip], o_send.at[0], o_recv.at[chip], {"tp_0": chip}
-        ).wait_recv()
+        for k in range(2):
+            view = landed.at[chip, k]
+            remote(view, view, o_send.at[0, k], o_recv.at[chip, k], {"tp_0": chip}).wait_recv()
     for chip in range(nx):
-        out_ref[:, chip * 2 * width : (chip + 1) * 2 * width] = landed[chip]
+        for k in range(2):
+            first = (chip * 2 + k) * width
+            out_ref[:, first : first + width] = landed[chip, k]
     for line in (along_y, along_z, wa, wb, wc, wd, one, two, three, spread_rows):
         line.drain()
     for copy in sent + posted + [w_over]:
@@ -607,12 +624,13 @@
             ((nz, 2 * part, width), BF16), ((nz, 2 * part, width), BF16),
             ((ny, 2 * part, width), BF16), ((ny, 2 * part, width), BF16),
             ((nt, own, width), BF16), ((nx, nt, own, width), BF16),
-            ((nx, own, 2 * width), BF16), ((nx, own, 2 * width), BF16),
+            ((nx * own, 2 * width), F32),
+            ((nx, 2, own, width), BF16), ((nx, 2, own, width), BF16),
         )
     ] + [
         dma(6), *pair(ny), *pair(nz), *pair(nt), *pair(GATHER_SEMS),
         *pair(ny), *pair(nz), *pair(nz), *pair(ny),
-        *pair(ny), *pair(nz), *pair(ny), dma(nx, 7), dma(nx, 7), *pair(nx), *pair(1),
+        *pair(ny), *pair(nz), *pair(ny), dma(nx, 7), dma(nx, 7), dma(nx, 2), dma(nx, 2), *pair(1),
     ]
     near = pl.BlockSpec(memory_space=pltpu.VMEM)
     return pl.pallas_call(

time: 65.5 us -> 65.2 us (level)
  no operation moved by 1% of the time
where the time goes in v6:
time: 65.2 us; the launch traced here: 64.2 us
  Pallas kernels  63.5 us (97%)
  local copies, waits for them, and re-layouts  0.71 us (1%)
    pallas_call x1, Pallas kernels, per_device(): pl.pallas_call(functools.partial(whole_kernel, sizes, ctx_len), out_shape...  63.5 us

profile of v6, /device:TPU:1, one launch (start us, length us, event | category | flops | bytes accessed | tf_op | source)
XLA Modules:
  0.0 64.2 jit_solution(12868966809611722248)
XLA Ops:
  0.0 63.5 %shard_map.145 = bf16[64,2048]{1,0:T(8,128)(2,1)S(1)} custom-call(f32[1,2048]{1,0:T(1,128)} %bitcast.6, f32[1,2048]{1,0:T(1,128)} %bitcast.7, bf16[3,32,256]{2,1,0:T(8,128)(2,1)} %bitcast.5, bf16[64,2048]{1,0:T(8,128)(2,1)} %lat_ref.1, bf16[16,2048]{1,0:T(8,128)(2,1)} %ctx_ref.1, bf16[32,2048]{1,0:T(8,128)(2,1)} %w_ref.1, f32[1,2048]{1,0:T(1,128)} %bitcast.8, ...), custom_call_target="tpu_custom_call" | custom-call | tf_op jit(solution)/shard_map/pallas_call | solution.py:636
  63.5 0.7 %copy.17 = bf16[64,2048]{1,0:T(8,128)(2,1)} copy(bf16[64,2048]{1,0:T(8,128)(2,1)S(1)} %shard_map.145) | data formatting | bytes 524288
